TPU v7x, 32 devices: a whole 2x2x4 slice. The times are simulated.
32 devices in a mesh: sp: 16 (over z, y, x), tp: 2 (over core).
Axes of the slice: x: 2, y: 2, z: 4, core: 2. Of those that a mesh axis runs over, the one named last changes fastest.
Arguments:
- stream: bfloat16 [7168, 2048], P('sp'), may hold values from -6 to 6
- norm_gain: float32 [2, 2048], replicated, may hold values from 0.1 to 1.9
- value_weight: bfloat16 [2, 2048, 512], P(None, None, 'tp'), may hold values from -0.125 to 0.125
- gate_weight: bfloat16 [2, 2048, 512], P(None, None, 'tp'), may hold values from -0.125 to 0.125
- conv_taps: bfloat16 [2, 512, 512], P(None, None, 'tp'), may hold values from -0.25 to 0.25
- conv_bias: float32 [2, 512], P(None, 'tp'), may hold values from -3 to 3
- channel_gain: float32 [2, 512], replicated, may hold values from 0.1 to 1.9
- channel_shift: float32 [2, 512], replicated, may hold values from -3 to 3
- out_weight: bfloat16 [2, 512, 2048], replicated, may hold values from -0.25 to 0.25
Outputs:
- result: bfloat16 [7168, 2048], P('sp')
All inputs are finite; a program needn't handle non-finite values.
Results may differ from a plain program's by a relative error of at most 0.0075.
Values may be sent and summed in bfloat16 or wider, within the bound.
No kernel may reach another device: no remote copies, remote signals or barrier semaphores. Data moves between devices by JAX's collectives and lax.ppermute only.
A program may use at most 64 MiB of HBM per device.

v0:
```python
import jax
import jax.numpy as jnp
from jax import lax
from jax.sharding import PartitionSpec as P


def passed_along(value, axis, by):
    count = lax.axis_size(axis)
    pairs = [(i, i + by) for i in range(count) if 0 <= i + by < count]
    return lax.ppermute(value, axis, pairs)


def rms_normed(stream, gain):
    values = stream.astype(jnp.float32)
    scale = lax.rsqrt(jnp.mean(values * values, axis=-1, keepdims=True) + 1e-06)
    return (values * scale * gain[None, :]).astype(jnp.bfloat16)


def channel_mix(conv, gain, shift):
    values = conv.astype(jnp.float32)
    center = jnp.mean(values, axis=-1, keepdims=True)
    spread = jnp.mean(jnp.square(values - center), axis=-1, keepdims=True)
    normed = (values - center) * lax.rsqrt(spread + 1e-05) * gain[None, :] + shift[None, :]
    return jax.nn.silu(normed).astype(jnp.bfloat16)


def gate_rows(normed, w_value, w_gate):
    values = jnp.dot(normed, w_value, preferred_element_type=jnp.float32)
    gates = jnp.dot(normed, w_gate, preferred_element_type=jnp.float32)
    return (values * jax.nn.sigmoid(gates)).astype(jnp.bfloat16)


def per_device(
    stream,
    norm_gain,
    value_weight,
    gate_weight,
    conv_taps,
    conv_bias,
    channel_gain,
    channel_shift,
    out_weight,
):
    tokens = stream.shape[0]
    reach = conv_taps.shape[1] - 1
    hops = -(-reach // tokens)
    state = stream
    for layer in range(norm_gain.shape[0]):
        normed = rms_normed(state, norm_gain[layer])
        own_gated = gate_rows(normed, value_weight[layer], gate_weight[layer])
        pieces = [own_gated]
        for step in range(1, hops + 1):
            count = min(tokens, reach - (step - 1) * tokens)
            pieces.insert(0, passed_along(own_gated[tokens - count :], "sp", step))
        gated = jnp.concatenate(pieces, axis=0)
        conv = lax.conv_general_dilated(
            gated[None],
            conv_taps[layer][:, None, :],
            (1,),
            [(0, 0)],
            dimension_numbers=("NWC", "WIO", "NWC"),
            feature_group_count=gated.shape[1],
            preferred_element_type=jnp.float32,
        )[0]
        conv = (conv + conv_bias[layer][None, :]).astype(jnp.bfloat16)
        every_channel = lax.all_gather(conv, "tp", axis=1, tiled=True)
        mixed = channel_mix(every_channel, channel_gain[layer], channel_shift[layer])
        update = jnp.dot(mixed, out_weight[layer], preferred_element_type=jnp.float32)
        state = (state.astype(jnp.float32) + update).astype(jnp.bfloat16)
    return state


def solution(mesh):
    return jax.shard_map(
        per_device,
        mesh=mesh,
        in_specs=(
            P("sp", None),
            P(),
            P(None, None, "tp"),
            P(None, None, "tp"),
            P(None, None, "tp"),
            P(None, "tp"),
            P(),
            P(),
            P(),
        ),
        out_specs=P("sp", None),
        check_vma=False,
    )
```

profile of v0, /device:TPU:25, one launch (start us, length us, event | category | flops | bytes accessed | tf_op | source)
XLA Modules:
  0.0 95.2 jit_solution(958022671761127983)
XLA Ops:
  0.0 1.9 %fusion = f32[448]{0:T(512)S(1)} fusion(bf16[448,2048]{1,0:T(8,128)(2,1)} %param.9), kind=kLoop, calls=%fused_computation.6 | loop fusion | flops 2752064 | bytes 1836800 | tf_op jit(solution)/shard_map/reduce_sum | solution.py:15
  1.9 0.8 fusion.76
  2.8 0.0 copy-start
  2.8 0.0 copy-start.7
  2.8 2.6 %fusion.17 = f32[448,256]{1,0:T(8,128)S(1)} fusion(bf16[2,2048,256]{2,1,0:T(8,128)(2,1)} %param.12, bf16[448,2048]{1,0:T(8,128)(2,1)} %param.9, f32[2048]{0:T(1024)S(1)} %bitcast.46, f32[448]{0:T(512)S(1)} %add_rsqrt_fusion.3), kind=kOutput, calls=%fused_computation.27 | convolution fusion | flops 473776128 | bytes 3352320 | tf_op jit(solution)/shard_map/dot_general | solution.py:29
  5.4 0.0 copy-done
  5.4 0.3 copy-done.7
  5.8 0.0 copy-start.2
  5.8 0.0 copy-start.1
  5.8 0.0 copy-start.3
  5.8 0.0 copy-start.4
  5.8 0.7 fusion.18
  6.5 3.1 %collective-permute-start.1 = (bf16[448,256]{1,0:T(8,128)(2,1)S(1)}, bf16[448,256]{1,0:T(8,128)(2,1)S(1)}, u32[]{:S(2)}, u32[]{:S(2)}) collective-permute-start(bf16[448,256]{1,0:T(8,128)(2,1)S(1)} %fusion.18), channel_id=1, source_target_pairs={{0,2},{2,4},{4,6},{6,8},{8,10},{10,12},{12,14},{14,16},{16,18},{18... | collective-permute-start | bytes 688136 | tf_op jit(solution)/shard_map/ppermute | solution.py:10
  9.7 3.1 %collective-permute-start = (bf16[63,256]{1,0:T(8,128)(2,1)S(1)}, bf16[63,256]{1,0:T(8,128)(2,1)S(1)}, u32[]{:S(2)}, u32[]{:S(2)}) collective-permute-start(bf16[63,256]{1,0:T(8,128)(2,1)S(1)} %slice.72), channel_id=1, source_target_pairs={{0,4},{2,6},{4,8},{6,10},{8,12},{10,14},{12,16},{14,18},{16,20},{1... | collective-permute-start | bytes 96776 | tf_op jit(solution)/shard_map/ppermute | solution.py:10
  12.8 0.0 copy-done.2
  12.8 0.0 copy-done.1
  12.9 0.0 copy-done.3
  12.9 0.0 copy-done.4
  12.9 3.5 %collective-permute-done = bf16[63,256]{1,0:T(8,128)(2,1)S(1)} collective-permute-done((bf16[63,256]{1,0:T(8,128)(2,1)S(1)}, bf16[63,256]{1,0:T(8,128)(2,1)S(1)}, u32[]{:S(2)}, u32[]{:S(2)}) %collective-permute-start) | collective-permute-done | bytes 32288 | tf_op jit(solution)/shard_map/ppermute | solution.py:10
  16.4 0.6 collective-permute-done.1
  17.0 0.1 maximum_bitcast_fusion
  17.1 0.0 copy-start.5
  17.1 26.7 %fusion.34 = f32[1,448,256]{2,0,1:T(1,128)S(1)} fusion(bf16[1,959,256]{2,1,0:T(8,128)(2,1)S(1)} %maximum_bitcast_fusion, bf16[512,1,256]{2,0,1:T(8,128)(2,1)S(1)} %get-tuple-element.6), kind=kOutput, calls=%fused_computation.48 | convolution fusion | flops 117440512 | bytes 1211904 | tf_op jit(solution)/shard_map/conv_general_dilated | solution.py:56
  43.9 3.7 %all_gather.6 = bf16[448,512]{1,0:T(8,128)(2,1)S(1)} all-gather(bf16[448,256]{1,0:T(8,128)(2,1)S(1)} %fusion.63), channel_id=1, replica_groups=mesh['sp'=16,'tp'=2] {'tp'}, dimensions={1}, use_global_device_ids=true | all-gather | bytes 688128 | tf_op jit(solution)/shard_map/all_gather | solution.py:66
  47.6 0.1 convert_reduce_fusion.1
  47.7 0.3 fusion.45
  48.0 0.0 copy-done.5
  48.0 0.0 copy-start.6
  48.1 1.7 %fusion.4 = (f32[448]{0:T(512)S(1)}, bf16[448,2048]{1,0:T(8,128)(2,1)S(1)}) fusion(bf16[2,512,2048]{2,1,0:T(8,128)(2,1)S(1)} %copy-done.5, bf16[448,512]{1,0:T(8,128)(2,1)S(1)} %all_gather.6, f32[512]{0:T(512)S(1)} %bitcast.53, f32[512]{0:T(512)S(1)} %bitcast.52, f32[448]{0:T(512)S(1)} %add_rsqrt_fusion.2, f32[448]{0:T(512)S(1)} %broadcast_multiply_fusion.1, ...), kind=kOutput, calls=%fused_computation.10 | convolution fusion | flops 947322432 | bytes 6235904 | tf_op jit(solution)/shard_map/dot_general | solution.py:68
  49.7 0.0 copy-done.6
  49.7 0.7 fusion.14
  50.5 0.7 fusion.19
  51.2 2.2 %collective-permute-start.3 = (bf16[448,256]{1,0:T(8,128)(2,1)S(1)}, bf16[448,256]{1,0:T(8,128)(2,1)S(1)}, u32[]{:S(2)}, u32[]{:S(2)}) collective-permute-start(bf16[448,256]{1,0:T(8,128)(2,1)S(1)} %fusion.19), channel_id=1, source_target_pairs={{0,2},{2,4},{4,6},{6,8},{8,10},{10,12},{12,14},{14,16},{16,18},{18... | collective-permute-start | bytes 688136 | tf_op jit(solution)/shard_map/ppermute | solution.py:10
  53.4 2.0 %collective-permute-start.2 = (bf16[63,256]{1,0:T(8,128)(2,1)S(1)}, bf16[63,256]{1,0:T(8,128)(2,1)S(1)}, u32[]{:S(2)}, u32[]{:S(2)}) collective-permute-start(bf16[63,256]{1,0:T(8,128)(2,1)S(1)} %slice.73), channel_id=1, source_target_pairs={{0,4},{2,6},{4,8},{6,10},{8,12},{10,14},{12,16},{14,18},{16,20},{1... | collective-permute-start | bytes 96776 | tf_op jit(solution)/shard_map/ppermute | solution.py:10
  55.4 4.8 %collective-permute-done.2 = bf16[63,256]{1,0:T(8,128)(2,1)S(1)} collective-permute-done((bf16[63,256]{1,0:T(8,128)(2,1)S(1)}, bf16[63,256]{1,0:T(8,128)(2,1)S(1)}, u32[]{:S(2)}, u32[]{:S(2)}) %collective-permute-start.2) | collective-permute-done | bytes 32288 | tf_op jit(solution)/shard_map/ppermute | solution.py:10
  60.2 1.9 %collective-permute-done.3 = bf16[448,256]{1,0:T(8,128)(2,1)S(1)} collective-permute-done((bf16[448,256]{1,0:T(8,128)(2,1)S(1)}, bf16[448,256]{1,0:T(8,128)(2,1)S(1)}, u32[]{:S(2)}, u32[]{:S(2)}) %collective-permute-start.3) | collective-permute-done | bytes 229408 | tf_op jit(solution)/shard_map/ppermute | solution.py:10
  62.1 0.1 maximum_bitcast_fusion.1
  62.2 26.6 %fusion.32 = f32[1,448,256]{2,0,1:T(1,128)S(1)} fusion(bf16[1,959,256]{2,1,0:T(8,128)(2,1)S(1)} %maximum_bitcast_fusion.1, bf16[512,1,256]{2,0,1:T(8,128)(2,1)S(1)} %get-tuple-element.5), kind=kOutput, calls=%fused_computation.46 | convolution fusion | flops 117440512 | bytes 1211904 | tf_op jit(solution)/shard_map/conv_general_dilated | solution.py:56
  88.9 3.3 %all_gather.7 = bf16[448,512]{1,0:T(8,128)(2,1)S(1)} all-gather(bf16[448,256]{1,0:T(8,128)(2,1)S(1)} %fusion.62), channel_id=1, replica_groups=mesh['sp'=16,'tp'=2] {'tp'}, dimensions={1}, use_global_device_ids=true | all-gather | bytes 688128 | tf_op jit(solution)/shard_map/all_gather | solution.py:66
  92.1 0.1 convert_reduce_fusion
  92.3 0.3 fusion.36
  92.6 2.6 %fusion.7 = bf16[448,2048]{1,0:T(8,128)(2,1)} fusion(bf16[448,2048]{1,0:T(8,128)(2,1)S(1)} %get-tuple-element.16, bf16[2,512,2048]{2,1,0:T(8,128)(2,1)S(1)} %copy-done.5, bf16[448,512]{1,0:T(8,128)(2,1)S(1)} %all_gather.7, f32[512]{0:T(512)S(1)} %bitcast.51, f32[512]{0:T(512)S(1)} %bitcast.50, f32[448]{0:T(512)S(1)} %add_rsqrt_fusion, ...), kind=kOutput, calls=%fused_computation.13 | convolution fusion | flops 944570368 | bytes 6234112 | tf_op jit(solution)/shard_map/dot_general | solution.py:68
  (14 shorter events, 0.2 us)
Async XLA Ops:
  2.8 2.7 %copy-start = (bf16[448,2048]{1,0:T(8,128)(2,1)S(1)}, bf16[448,2048]{1,0:T(8,128)(2,1)}, u32[]{:S(2)}) copy-start(bf16[448,2048]{1,0:T(8,128)(2,1)} %param.9) | copy-start | bytes 5505028
  2.8 3.0 %copy-start.7 = (bf16[2,2048,256]{2,1,0:T(8,128)(2,1)S(1)}, bf16[2,2048,256]{2,1,0:T(8,128)(2,1)}, u32[]{:S(2)}) copy-start(bf16[2,2048,256]{2,1,0:T(8,128)(2,1)} %param.11) | copy-start | bytes 6291460
  5.8 7.0 %copy-start.2 = (f32[2,512]{1,0:T(2,128)S(1)}, f32[2,512]{1,0:T(2,128)}, u32[]{:S(2)}) copy-start(f32[2,512]{1,0:T(2,128)} %param.15) | copy-start | bytes 12292
  5.8 7.1 %copy-start.1 = (bf16[2,512,256]{2,1,0:T(8,128)(2,1)S(1)}, bf16[2,512,256]{2,1,0:T(8,128)(2,1)}, u32[]{:S(2)}) copy-start(bf16[2,512,256]{2,1,0:T(8,128)(2,1)} %param.13) | copy-start | bytes 1572868
  5.8 7.1 %copy-start.3 = (f32[2,512]{1,0:T(2,128)S(1)}, f32[2,512]{1,0:T(2,128)}, u32[]{:S(2)}) copy-start(f32[2,512]{1,0:T(2,128)} %param.16) | copy-start | bytes 12292
  5.8 7.1 %copy-start.4 = (f32[2,256]{1,0:T(2,128)S(1)}, f32[2,256]{1,0:T(2,128)}, u32[]{:S(2)}) copy-start(f32[2,256]{1,0:T(2,128)} %param.14) | copy-start | bytes 6148
  6.5 10.5 %collective-permute-start.1 = (bf16[448,256]{1,0:T(8,128)(2,1)S(1)}, bf16[448,256]{1,0:T(8,128)(2,1)S(1)}, u32[]{:S(2)}, u32[]{:S(2)}) collective-permute-start(bf16[448,256]{1,0:T(8,128)(2,1)S(1)} %fusion.18), channel_id=1, source_target_pairs={{0,2},{2,4},{4,6},{6,8},{8,10},{10,12},{12,14},{14,16},{16,18},{18... | collective-permute-start | bytes 688136 | tf_op jit(solution)/shard_map/ppermute | solution.py:10
  9.7 6.8 %collective-permute-start = (bf16[63,256]{1,0:T(8,128)(2,1)S(1)}, bf16[63,256]{1,0:T(8,128)(2,1)S(1)}, u32[]{:S(2)}, u32[]{:S(2)}) collective-permute-start(bf16[63,256]{1,0:T(8,128)(2,1)S(1)} %slice.72), channel_id=1, source_target_pairs={{0,4},{2,6},{4,8},{6,10},{8,12},{10,14},{12,16},{14,18},{16,20},{1... | collective-permute-start | bytes 96776 | tf_op jit(solution)/shard_map/ppermute | solution.py:10
  17.1 30.9 %copy-start.5 = (bf16[2,512,2048]{2,1,0:T(8,128)(2,1)S(1)}, bf16[2,512,2048]{2,1,0:T(8,128)(2,1)}, u32[]{:S(2)}) copy-start(bf16[2,512,2048]{2,1,0:T(8,128)(2,1)} %param.17) | copy-start | bytes 12582916
  48.0 1.7 %copy-start.6 = (bf16[2,2048,256]{2,1,0:T(8,128)(2,1)S(1)}, bf16[2,2048,256]{2,1,0:T(8,128)(2,1)}, u32[]{:S(2)}) copy-start(bf16[2,2048,256]{2,1,0:T(8,128)(2,1)} %param.12) | copy-start | bytes 6291460
  51.2 10.9 %collective-permute-start.3 = (bf16[448,256]{1,0:T(8,128)(2,1)S(1)}, bf16[448,256]{1,0:T(8,128)(2,1)S(1)}, u32[]{:S(2)}, u32[]{:S(2)}) collective-permute-start(bf16[448,256]{1,0:T(8,128)(2,1)S(1)} %fusion.19), channel_id=1, source_target_pairs={{0,2},{2,4},{4,6},{6,8},{8,10},{10,12},{12,14},{14,16},{16,18},{18... | collective-permute-start | bytes 688136 | tf_op jit(solution)/shard_map/ppermute | solution.py:10
  53.4 6.8 %collective-permute-start.2 = (bf16[63,256]{1,0:T(8,128)(2,1)S(1)}, bf16[63,256]{1,0:T(8,128)(2,1)S(1)}, u32[]{:S(2)}, u32[]{:S(2)}) collective-permute-start(bf16[63,256]{1,0:T(8,128)(2,1)S(1)} %slice.73), channel_id=1, source_target_pairs={{0,4},{2,6},{4,8},{6,10},{8,12},{10,14},{12,16},{14,18},{16,20},{1... | collective-permute-start | bytes 96776 | tf_op jit(solution)/shard_map/ppermute | solution.py:10
where the time goes:
time: 95.7 us; the launch traced here: 95.2 us
  matrix products  62.4 us (65%)
  waiting for transfers between devices  10.8 us (11%)
  starting transfers between devices  10.4 us (11%)
  blocking collectives  6.95 us (7%)
  other arithmetic  3.19 us (3%)
  local copies, waits for them, and re-layouts  1.27 us (1%)
    conv_general_dilated x2, matrix products, per_device(): lax.conv_general_dilated(gated[None], conv_taps[layer][:, None, :], (1,),...  53.3 us
    ppermute x4, waiting for transfers between devices, passed_along(): return lax.ppermute(value, axis, pairs)  10.8 us
    ppermute x4, starting transfers between devices, passed_along(): return lax.ppermute(value, axis, pairs)  10.4 us
    all_gather x2, blocking collectives, per_device(): every_channel = lax.all_gather(conv, 'tp', axis=1, tiled=True)  6.95 us
    dot_general x2, matrix products, per_device(): jnp.dot(mixed, out_weight[layer], preferred_element_type=jnp.float32)  4.29 us
    dot_general x2, matrix products, gate_rows(): gates = jnp.dot(normed, w_gate, preferred_element_type=jnp.float32)  3.35 us
    reduce_sum x1, other arithmetic, rms_normed(): scale = lax.rsqrt(jnp.mean(values * values, axis=-1, keepdims=True) + 1e-06)  1.94 us
  transfers between devices with their start and end apart: 4, of which 4 were waited for; matrix products, arithmetic and copies ran while one was open for 0% of the time, Pallas kernels for 0%

commit v1 on v0

--- a/solution.py
+++ b/solution.py
@@ -1,7 +1,14 @@
+import functools
+
 import jax
 import jax.numpy as jnp
+import numpy as np
 from jax import lax
+from jax.experimental import pallas as pl
+from jax.experimental.pallas import tpu as pltpu
 from jax.sharding import PartitionSpec as P
+
+STEP = 32
 
 
 def passed_along(value, axis, by):
@@ -28,6 +35,87 @@
     values = jnp.dot(normed, w_value, preferred_element_type=jnp.float32)
     gates = jnp.dot(normed, w_gate, preferred_element_type=jnp.float32)
     return (values * jax.nn.sigmoid(gates)).astype(jnp.bfloat16)
+
+
+def rotations(rows, cols, row_at, col_at, unit, scale):
+    col = col_at(np.arange(cols, dtype=np.float64))
+    coarse = row_at(np.arange(0, rows, STEP, dtype=np.float64))
+    fine = row_at(np.arange(STEP, dtype=np.float64)) - row_at(np.float64(0))
+    a = unit * np.outer(coarse, col)
+    b = unit * np.outer(fine, col)
+    both = [scale * np.cos(a), scale * np.sin(a), np.cos(b), np.sin(b)]
+    return [x.astype(np.float32) for x in both]
+
+
+def split(value, hi_ref, lo_ref, rows):
+    hi = value.astype(jnp.bfloat16)
+    hi_ref[rows, :] = hi
+    lo_ref[rows, :] = (value - hi.astype(jnp.float32)).astype(jnp.bfloat16)
+
+
+def spread_out(tables, outs):
+    ca, sa, cb, sb = tables
+    c_hi, c_lo, s_hi, s_lo = outs
+
+    for i in range(ca.shape[0]):
+        rows = pl.ds(i * STEP, STEP)
+        c1 = ca[i : i + 1, :]
+        s1 = sa[i : i + 1, :]
+        c2 = cb[...]
+        s2 = sb[...]
+        split(c1 * c2 - s1 * s2, c_hi, c_lo, rows)
+        split(s1 * c2 + c1 * s2, s_hi, s_lo, rows)
+
+
+def dot(a, b):
+    return jnp.dot(a, b, preferred_element_type=jnp.float32)
+
+
+def prep_kernel(*refs):
+    own_t, halo_t, back_t = refs[0:4], refs[4:8], refs[8:12]
+    taps = refs[12]
+    own, halo, back = refs[13:17], refs[17:21], refs[21:25]
+    tap_c, tap_s = refs[25:27]
+    spread_out(halo_t, halo)
+    for layer in range(taps.shape[0]):
+        t = taps[layer]
+        tap_c[layer] = dot(halo[0][...], t) + dot(halo[1][...], t)
+        tap_s[layer] = dot(halo[2][...], t) + dot(halo[3][...], t)
+    spread_out(own_t, own)
+    spread_out(back_t, back)
+
+
+def own_kernel(c_hi, c_lo, s_hi, s_lo, gated, w_c, w_s):
+    g = gated[...]
+    w_c[...] = dot(c_hi[...], g) + dot(c_lo[...], g)
+    w_s[...] = dot(s_hi[...], g) + dot(s_lo[...], g)
+
+
+def parts(value):
+    hi = value.astype(jnp.bfloat16)
+    return hi, (value - hi.astype(jnp.float32)).astype(jnp.bfloat16)
+
+
+def finish_kernel(*refs, layer, pieces):
+    halo, back = refs[0:4], refs[4:8]
+    tap_c, tap_s, own_c, own_s, bias = refs[8:13]
+    got = refs[13 : 13 + pieces]
+    out = refs[13 + pieces]
+    window = jnp.concatenate([g[...] for g in got], axis=0)
+    w_c = own_c[...] + dot(halo[0][...], window) + dot(halo[1][...], window)
+    w_s = own_s[...] + dot(halo[2][...], window) + dot(halo[3][...], window)
+    h_c = tap_c[layer]
+    h_s = tap_s[layer]
+    re_hi, re_lo = parts(w_c * h_c + w_s * h_s)
+    im_hi, im_lo = parts(w_s * h_c - w_c * h_s)
+    y = dot(back[0][...], re_hi) + dot(back[2][...], im_hi)
+    y += dot(back[1][...], re_hi) + dot(back[3][...], im_hi)
+    y += dot(back[0][...], re_lo) + dot(back[2][...], im_lo)
+    out[...] = (y + bias[layer : layer + 1, :]).astype(jnp.bfloat16)
+
+
+def cost(flops, size):
+    return pl.CostEstimate(flops=flops, bytes_accessed=size, transcendentals=0)
 
 
 def per_device(
@@ -42,27 +130,56 @@
     out_weight,
 ):
     tokens = stream.shape[0]
-    reach = conv_taps.shape[1] - 1
-    hops = -(-reach // tokens)
+    layers, width, chans = conv_taps.shape
+    halo_rows = -(-(width - 1) // 16) * 16
+    hops = -(-halo_rows // tokens)
+    size = -(-(tokens + halo_rows) // (2 * STEP)) * (2 * STEP)
+    half = size // 2
+    unit = 2 * np.pi / size
+    bf16, f32 = jnp.bfloat16, jnp.float32
+    assert tokens % STEP == 0 and halo_rows >= width
+
+    def freq(k):
+        return k + 0.5
+
+    own_tab = rotations(half, tokens, freq, lambda t: t + 1, unit, 1.0)
+    halo_tab = rotations(half, halo_rows, freq, lambda i: i + 1 - halo_rows, unit, 1.0)
+    back_tab = rotations(tokens, half, lambda t: t + 1, freq, unit, 2.0 / size)
+    taps = conv_taps
+    if halo_rows > width:
+        taps = jnp.pad(conv_taps, ((0, 0), (halo_rows - width, 0), (0, 0)))
+
+    mats = [(half, tokens)] * 4 + [(half, halo_rows)] * 4 + [(tokens, half)] * 4
+    shapes = [jax.ShapeDtypeStruct(m, bf16) for m in mats]
+    shapes += [jax.ShapeDtypeStruct((layers, half, chans), f32)] * 2
+    made = pl.pallas_call(
+        prep_kernel,
+        out_shape=shapes,
+        cost_estimate=cost(4 * layers * size * halo_rows * chans, 8 << 20),
+        name="prep",
+    )(*own_tab, *halo_tab, *back_tab, taps)
+    own_m, halo_m, back_m, tap_f = made[0:4], made[4:8], made[8:12], made[12:14]
+
     state = stream
-    for layer in range(norm_gain.shape[0]):
+    for layer in range(layers):
         normed = rms_normed(state, norm_gain[layer])
         own_gated = gate_rows(normed, value_weight[layer], gate_weight[layer])
-        pieces = [own_gated]
+        pieces = []
         for step in range(1, hops + 1):
-            count = min(tokens, reach - (step - 1) * tokens)
+            count = min(tokens, halo_rows - (step - 1) * tokens)
             pieces.insert(0, passed_along(own_gated[tokens - count :], "sp", step))
-        gated = jnp.concatenate(pieces, axis=0)
-        conv = lax.conv_general_dilated(
-            gated[None],
-            conv_taps[layer][:, None, :],
-            (1,),
-            [(0, 0)],
-            dimension_numbers=("NWC", "WIO", "NWC"),
-            feature_group_count=gated.shape[1],
-            preferred_element_type=jnp.float32,
-        )[0]
-        conv = (conv + conv_bias[layer][None, :]).astype(jnp.bfloat16)
+        own_f = pl.pallas_call(
+            own_kernel,
+            out_shape=[jax.ShapeDtypeStruct((half, chans), f32)] * 2,
+            cost_estimate=cost(4 * size * tokens * chans, 4 << 20),
+            name="own_part",
+        )(*own_m, own_gated)
+        conv = pl.pallas_call(
+            functools.partial(finish_kernel, layer=layer, pieces=len(pieces)),
+            out_shape=jax.ShapeDtypeStruct((tokens, chans), bf16),
+            cost_estimate=cost(4 * size * halo_rows * chans, 4 << 20),
+            name="finish",
+        )(*halo_m, *back_m, *tap_f, *own_f, conv_bias, *pieces)
         every_channel = lax.all_gather(conv, "tp", axis=1, tiled=True)
         mixed = channel_mix(every_channel, channel_gain[layer], channel_shift[layer])
         update = jnp.dot(mixed, out_weight[layer], preferred_element_type=jnp.float32)

time: 95.7 us -> 65.7 us (0.69)
  matrix products: 62.4 us -> 12.3 us
  Pallas kernels: 0 us -> 24.7 us
  waiting for transfers between devices: 10.8 us -> 4.01 us
  local copies, waits for them, and re-layouts: 1.27 us -> 4.1 us
    conv_general_dilated x2 -> x0, matrix products: 53.3 us -> none  [per_device(): lax.conv_general_dilated(gated[None], conv_taps[layer][:, None, :], (1,),...]
    pallas_call x0 -> x5, Pallas kernels: none -> 24.7 us  [the longest x2 12.5 us: per_device(): pl.pallas_call(functools.partial(finish_kernel, layer=layer, pieces=len(p...]
    ppermute x4, waiting for transfers between devices: 10.8 us -> 4.01 us  [passed_along(): return lax.ppermute(value, axis, pairs)]
    dot_general x2, matrix products: 4.29 us -> 7.52 us  [per_device(): jnp.dot(mixed, out_weight[layer], preferred_element_type=jnp.float32)]
    unnamed x16 -> x28, local copies, waits for them, and re-layouts: 0.38 us -> 3.26 us
  transfers between devices with their start and end apart: 4 -> 4, of which waited for: 4 -> 2; matrix products, arithmetic and copies ran while one was open for 0% -> 0% of each run, Pallas kernels for 0% -> 19%
where the time goes in v1:
time: 65.7 us; the launch traced here: 65.2 us
  Pallas kernels  24.7 us (38%)
  matrix products  12.3 us (19%)
  starting transfers between devices  10.2 us (16%)
  blocking collectives  6.76 us (10%)
  local copies, waits for them, and re-layouts  4.1 us (6%)
  waiting for transfers between devices  4.01 us (6%)
  other arithmetic  2.88 us (4%)
    pallas_call x2, Pallas kernels, per_device(): pl.pallas_call(functools.partial(finish_kernel, layer=layer, pieces=len(p...  12.5 us
    ppermute x4, starting transfers between devices, passed_along(): return lax.ppermute(value, axis, pairs)  10.2 us
    dot_general x2, matrix products, per_device(): jnp.dot(mixed, out_weight[layer], preferred_element_type=jnp.float32)  7.52 us
    all_gather x2, blocking collectives, per_device(): every_channel = lax.all_gather(conv, 'tp', axis=1, tiled=True)  6.76 us
    pallas_call x2, Pallas kernels, per_device(): pl.pallas_call(own_kernel, out_shape=[jax.ShapeDtypeStruct((half, chans),...  6.32 us
    pallas_call x1, Pallas kernels, per_device(): pl.pallas_call(prep_kernel, out_shape=shapes, cost_estimate=cost(4 * laye...  5.78 us
    ppermute x4, waiting for transfers between devices, passed_along(): return lax.ppermute(value, axis, pairs)  4.01 us
    dot_general x2, matrix products, gate_rows(): gates = jnp.dot(normed, w_gate, preferred_element_type=jnp.float32)  3.35 us
  transfers between devices with their start and end apart: 4, of which 2 were waited for; matrix products, arithmetic and copies ran while one was open for 0% of the time, Pallas kernels for 19%

profile of v1, /device:TPU:25, one launch (start us, length us, event | category | flops | bytes accessed | tf_op | source)
XLA Modules:
  0.0 65.2 jit_solution(8277493548969941110)
XLA Ops:
  0.0 1.9 %fusion = f32[448]{0:T(512)S(1)} fusion(bf16[448,2048]{1,0:T(8,128)(2,1)} %param.21), kind=kLoop, calls=%fused_computation.6 | loop fusion | flops 2752064 | bytes 1836800 | tf_op jit(solution)/shard_map/reduce_sum | solution.py:22
  1.9 0.8 %fusion.68 = (f32[1,2048]{1,0:T(1,128)S(1)}, f32[1,2048]{1,0:T(1,128)S(1)}) fusion(f32[2,2048]{1,0:T(2,128)} %param.22), kind=kLoop, calls=%fused_computation.82 | loop fusion | bytes 32768 | tf_op jit(solution)/shard_map/slice | solution.py:165
  2.8 0.0 copy-start
  2.8 0.0 copy-start.10
  2.8 2.6 %fusion.17 = f32[448,256]{1,0:T(8,128)S(1)} fusion(bf16[2,2048,256]{2,1,0:T(8,128)(2,1)} %param.24, bf16[448,2048]{1,0:T(8,128)(2,1)} %param.21, f32[2048]{0:T(1024)S(1)} %bitcast.28, f32[448]{0:T(512)S(1)} %add_rsqrt_fusion.3), kind=kOutput, calls=%fused_computation.27 | convolution fusion | flops 473776128 | bytes 3352320 | tf_op jit(solution)/shard_map/dot_general | solution.py:36
  5.4 0.0 copy-done
  5.4 0.3 copy-done.10
  5.8 0.0 copy-start.7
  5.8 0.7 %fusion.18.gated = bf16[448,256]{1,0:T(8,128)(2,1)S(1)} fusion(f32[448,256]{1,0:T(8,128)S(1)} %fusion.17, bf16[2,2048,256]{2,1,0:T(8,128)(2,1)S(1)} %copy-done.10, bf16[448,2048]{1,0:T(8,128)(2,1)S(1)} %copy-done, f32[2048]{0:T(1024)S(1)} %bitcast.29, f32[448]{0:T(512)S(1)} %add_rsqrt_fusion.3), kind=kOutput, calls=%fused_computation.28 | convolution fusion | flops 473661440 | bytes 3581952 | tf_op jit(solution)/shard_map/dot_general | solution.py:35
  6.5 0.0 copy-start.1
  6.5 0.0 copy-start.8
  6.5 3.3 %collective-permute-start.1 = (bf16[448,256]{1,0:T(8,128)(2,1)S(1)}, bf16[448,256]{1,0:T(8,128)(2,1)S(1)}, u32[]{:S(2)}, u32[]{:S(2)}) collective-permute-start(bf16[448,256]{1,0:T(8,128)(2,1)S(1)} %fusion.18.gated), channel_id=1, source_target_pairs={{0,2},{2,4},{4,6},{6,8},{8,10},{10,12},{12,14},{14,16},{16,18},{18... | collective-permute-start | bytes 688136 | tf_op jit(solution)/shard_map/ppermute | solution.py:17
  9.8 3.1 %collective-permute-start = (bf16[64,256]{1,0:T(8,128)(2,1)S(1)}, bf16[64,256]{1,0:T(8,128)(2,1)S(1)}, u32[]{:S(2)}, u32[]{:S(2)}) collective-permute-start(bf16[64,256]{1,0:T(8,128)(2,1)S(1)} %slice.56), channel_id=1, source_target_pairs={{0,4},{2,6},{4,8},{6,10},{8,12},{10,14},{12,16},{14,18},{16,20},{1... | collective-permute-start | bytes 98312 | tf_op jit(solution)/shard_map/ppermute | solution.py:17
  12.9 0.0 copy-done.7
  13.0 5.8 %prep.1 = (bf16[480,448]{1,0:T(8,128)(2,1)}, bf16[480,448]{1,0:T(8,128)(2,1)}, bf16[480,448]{1,0:T(8,128)(2,1)}, bf16[480,448]{1,0:T(8,128)(2,1)}, bf16[480,512]...) custom-call(f32[15,448]{1,0:T(8,128)} %constant.45.clone.refs_0_, ...), custom_call_target="tpu_custom_call" | custom-call | flops 1006632960 | bytes 8388608 | tf_op jit(solution)/shard_map/prep/pallas_call | solution.py:155
  18.7 0.0 copy-done.8
  18.8 0.0 copy-done.1
  18.8 3.1 %own_part.2 = (f32[480,256]{1,0:T(8,128)}, f32[480,256]{1,0:T(8,128)}) custom-call(bf16[480,448]{1,0:T(8,128)(2,1)} %get-tuple-element.33.c_hi, bf16[480,448]{1,0:T(8,128)(2,1)} %get-tuple-element.34.c_lo, bf16[480,448]{1,0:T(8,128)(2,1)} %get-tuple-element.35.s_hi, bf16[480,448]{1,0:T(8,128)(2,1)} %get-tuple-element.36.s_lo, bf16[448,256]{1,0:T(8,128)(2,1)} %copy-done.1), custom_call_target="tpu_custom_call" | custom-call | flops 440401920 | bytes 4194304 | tf_op jit(solution)/shard_map/own_part/pallas_call | solution.py:171
  21.9 0.0 collective-permute-done.refs_13_
  21.9 0.0 copy-start.5
  21.9 0.0 collective-permute-done.1.refs_14_
  21.9 0.0 copy-start.3
  21.9 0.6 copy-done.5
  22.5 0.1 copy-done.3
  22.6 6.2 %finish.2 = bf16[448,256]{1,0:T(8,128)(2,1)} custom-call(bf16[480,512]{1,0:T(8,128)(2,1)} %get-tuple-element.23.refs_0_, bf16[480,512]{1,0:T(8,128)(2,1)} %get-tuple-element.24.refs_1_, bf16[480,512]{1,0:T(8,128)(2,1)} %get-tuple-element.25.refs_2_, bf16[480,512]{1,0:T(8,128)(2,1)} %get-tuple-element.26.refs_3_, bf16[448,480]{1,0:T(8,128)(2,1)} %get-tuple-element.27.refs_4_, ...), custom_call_target="tpu_custom_call" | custom-call | flops 503316480 | bytes 4194304 | tf_op jit(solution)/shard_map/finish/pallas_call | solution.py:177
  28.8 3.2 %all_gather.6 = bf16[448,512]{1,0:T(8,128)(2,1)S(1)} all-gather(bf16[448,256]{1,0:T(8,128)(2,1)} %finish.2), channel_id=1, replica_groups=mesh['sp'=16,'tp'=2] {'tp'}, dimensions={1}, use_global_device_ids=true | all-gather | bytes 688128 | tf_op jit(solution)/shard_map/all_gather | solution.py:183
  32.0 0.1 convert_reduce_fusion.1
  32.2 0.3 fusion.41
  32.5 0.0 copy-start.9
  32.5 3.3 %fusion.4 = (f32[448]{0:T(512)S(1)}, bf16[448,2048]{1,0:T(8,128)(2,1)S(1)}) fusion(bf16[2,512,2048]{2,1,0:T(8,128)(2,1)} %param.29, bf16[448,512]{1,0:T(8,128)(2,1)S(1)} %all_gather.6, f32[512]{0:T(512)S(1)} %bitcast.33, f32[512]{0:T(512)S(1)} %bitcast.32, f32[448]{0:T(512)S(1)} %add_rsqrt_fusion.2, f32[448]{0:T(512)S(1)} %broadcast_multiply_fusion.1, ...), kind=kOutput, calls=%fused_computation.10 | convolution fusion | flops 947322432 | bytes 6235392 | tf_op jit(solution)/shard_map/dot_general | solution.py:185
  35.8 0.0 copy-start.12
  35.8 0.0 copy-done.9
  35.9 0.0 copy-start.11
  35.9 0.7 %fusion.14 = f32[448,256]{1,0:T(8,128)S(1)} fusion(bf16[2,2048,256]{2,1,0:T(8,128)(2,1)S(1)} %copy-done.9, bf16[448,2048]{1,0:T(8,128)(2,1)S(1)} %get-tuple-element.48, f32[2048]{0:T(1024)S(1)} %bitcast.26, f32[448]{0:T(512)S(1)} %add_rsqrt_fusion.1), kind=kOutput, calls=%fused_computation.23 | convolution fusion | flops 473776128 | bytes 3352576 | tf_op jit(solution)/shard_map/dot_general | solution.py:36
  36.6 0.5 copy-done.12
  37.1 1.0 %copy-done.11 = bf16[2,2048,256]{2,1,0:T(8,128)(2,1)S(1)} copy-done((bf16[2,2048,256]{2,1,0:T(8,128)(2,1)S(1)}, bf16[2,2048,256]{2,1,0:T(8,128)(2,1)}, u32[]{:S(2)}) %copy-start.11) | copy-done | bytes 2097176
  38.1 0.7 %fusion.19.gated = bf16[448,256]{1,0:T(8,128)(2,1)S(1)} fusion(f32[448,256]{1,0:T(8,128)S(1)} %fusion.14, bf16[2,2048,256]{2,1,0:T(8,128)(2,1)S(1)} %copy-done.11, bf16[448,2048]{1,0:T(8,128)(2,1)S(1)} %get-tuple-element.48, f32[2048]{0:T(1024)S(1)} %bitcast.27, f32[448]{0:T(512)S(1)} %add_rsqrt_fusion.1), kind=kOutput, calls=%fused_computation.29 | convolution fusion | flops 473661440 | bytes 3581952 | tf_op jit(solution)/shard_map/dot_general | solution.py:35
  38.8 0.0 copy-start.2
  38.8 1.9 %collective-permute-start.3 = (bf16[448,256]{1,0:T(8,128)(2,1)S(1)}, bf16[448,256]{1,0:T(8,128)(2,1)S(1)}, u32[]{:S(2)}, u32[]{:S(2)}) collective-permute-start(bf16[448,256]{1,0:T(8,128)(2,1)S(1)} %fusion.19.gated), channel_id=1, source_target_pairs={{0,2},{2,4},{4,6},{6,8},{8,10},{10,12},{12,14},{14,16},{16,18},{18... | collective-permute-start | bytes 688136 | tf_op jit(solution)/shard_map/ppermute | solution.py:17
  40.8 1.9 %collective-permute-start.2 = (bf16[64,256]{1,0:T(8,128)(2,1)S(1)}, bf16[64,256]{1,0:T(8,128)(2,1)S(1)}, u32[]{:S(2)}, u32[]{:S(2)}) collective-permute-start(bf16[64,256]{1,0:T(8,128)(2,1)S(1)} %slice.57), channel_id=1, source_target_pairs={{0,4},{2,6},{4,8},{6,10},{8,12},{10,14},{12,16},{14,18},{16,20},{1... | collective-permute-start | bytes 98312 | tf_op jit(solution)/shard_map/ppermute | solution.py:17
  42.7 0.0 copy-done.2
  42.7 3.2 %own_part.3 = (f32[480,256]{1,0:T(8,128)}, f32[480,256]{1,0:T(8,128)}) custom-call(bf16[480,448]{1,0:T(8,128)(2,1)} %get-tuple-element.33.c_hi, bf16[480,448]{1,0:T(8,128)(2,1)} %get-tuple-element.34.c_lo, bf16[480,448]{1,0:T(8,128)(2,1)} %get-tuple-element.35.s_hi, bf16[480,448]{1,0:T(8,128)(2,1)} %get-tuple-element.36.s_lo, bf16[448,256]{1,0:T(8,128)(2,1)} %copy-done.2), custom_call_target="tpu_custom_call" | custom-call | flops 440401920 | bytes 4194304 | tf_op jit(solution)/shard_map/own_part/pallas_call | solution.py:171
  45.9 0.8 %collective-permute-done.2.refs_13_ = bf16[64,256]{1,0:T(8,128)(2,1)S(1)} collective-permute-done((bf16[64,256]{1,0:T(8,128)(2,1)S(1)}, bf16[64,256]{1,0:T(8,128)(2,1)S(1)}, u32[]{:S(2)}, u32[]{:S(2)}) %collective-permute-start.2) | collective-permute-done | bytes 32800 | tf_op jit(solution)/shard_map/ppermute | solution.py:17
  46.7 0.0 copy-start.6
  46.7 3.2 %collective-permute-done.3.refs_14_ = bf16[448,256]{1,0:T(8,128)(2,1)S(1)} collective-permute-done((bf16[448,256]{1,0:T(8,128)(2,1)S(1)}, bf16[448,256]{1,0:T(8,128)(2,1)S(1)}, u32[]{:S(2)}, u32[]{:S(2)}) %collective-permute-start.3) | collective-permute-done | bytes 229408 | tf_op jit(solution)/shard_map/ppermute | solution.py:17
  49.9 0.0 copy-start.4
  49.9 0.0 copy-done.6
  49.9 0.7 %copy-done.4 = bf16[448,256]{1,0:T(8,128)(2,1)} copy-done((bf16[448,256]{1,0:T(8,128)(2,1)}, bf16[448,256]{1,0:T(8,128)(2,1)S(1)}, u32[]{:S(2)}) %copy-start.4) | copy-done | bytes 229400
  50.6 0.0 copy-start.13
  50.6 6.3 %finish.3 = bf16[448,256]{1,0:T(8,128)(2,1)} custom-call(bf16[480,512]{1,0:T(8,128)(2,1)} %get-tuple-element.23.refs_0_, bf16[480,512]{1,0:T(8,128)(2,1)} %get-tuple-element.24.refs_1_, bf16[480,512]{1,0:T(8,128)(2,1)} %get-tuple-element.25.refs_2_, bf16[480,512]{1,0:T(8,128)(2,1)} %get-tuple-element.26.refs_3_, bf16[448,480]{1,0:T(8,128)(2,1)} %get-tuple-element.27.refs_4_, ...), custom_call_target="tpu_custom_call" | custom-call | flops 503316480 | bytes 4194304 | tf_op jit(solution)/shard_map/finish/pallas_call | solution.py:177
  56.9 3.6 %all_gather.7 = bf16[448,512]{1,0:T(8,128)(2,1)S(1)} all-gather(bf16[448,256]{1,0:T(8,128)(2,1)} %finish.3), channel_id=1, replica_groups=mesh['sp'=16,'tp'=2] {'tp'}, dimensions={1}, use_global_device_ids=true | all-gather | bytes 688128 | tf_op jit(solution)/shard_map/all_gather | solution.py:183
  60.5 0.1 convert_reduce_fusion
  60.6 0.3 fusion.32
  60.9 0.0 copy-done.13
  60.9 4.2 %fusion.7 = bf16[448,2048]{1,0:T(8,128)(2,1)} fusion(bf16[448,2048]{1,0:T(8,128)(2,1)S(1)} %copy-done.13, bf16[2,512,2048]{2,1,0:T(8,128)(2,1)} %param.29, bf16[448,512]{1,0:T(8,128)(2,1)S(1)} %all_gather.7, f32[512]{0:T(512)S(1)} %bitcast.31, f32[512]{0:T(512)S(1)} %bitcast.30, f32[448]{0:T(512)S(1)} %add_rsqrt_fusion, f32[448]{0:T(512)S(1)} %broadcast_multiply_fusion), kind=kOutput, calls=%fused_computation.13 | convolution fusion | flops 944570368 | bytes 6233600 | tf_op jit(solution)/shard_map/dot_general | solution.py:185
  (10 shorter events, 0.1 us)
Async XLA Ops:
  2.8 2.7 %copy-start = (bf16[448,2048]{1,0:T(8,128)(2,1)S(1)}, bf16[448,2048]{1,0:T(8,128)(2,1)}, u32[]{:S(2)}) copy-start(bf16[448,2048]{1,0:T(8,128)(2,1)} %param.21) | copy-start | bytes 5505028
  2.8 3.0 %copy-start.10 = (bf16[2,2048,256]{2,1,0:T(8,128)(2,1)S(1)}, bf16[2,2048,256]{2,1,0:T(8,128)(2,1)}, u32[]{:S(2)}) copy-start(bf16[2,2048,256]{2,1,0:T(8,128)(2,1)} %param.23) | copy-start | bytes 6291460
  5.8 7.2 %copy-start.7 = (f32[2,512]{1,0:T(2,128)S(1)}, f32[2,512]{1,0:T(2,128)}, u32[]{:S(2)}) copy-start(f32[2,512]{1,0:T(2,128)} %param.27) | copy-start | bytes 12292
  6.5 12.3 %copy-start.1 = (bf16[448,256]{1,0:T(8,128)(2,1)}, bf16[448,256]{1,0:T(8,128)(2,1)S(1)}, u32[]{:S(2)}) copy-start(bf16[448,256]{1,0:T(8,128)(2,1)S(1)} %fusion.18.gated) | copy-start | bytes 688132
  6.5 12.3 %copy-start.8 = (f32[2,512]{1,0:T(2,128)S(1)}, f32[2,512]{1,0:T(2,128)}, u32[]{:S(2)}) copy-start(f32[2,512]{1,0:T(2,128)} %param.28) | copy-start | bytes 12292
  6.5 15.4 %collective-permute-start.1 = (bf16[448,256]{1,0:T(8,128)(2,1)S(1)}, bf16[448,256]{1,0:T(8,128)(2,1)S(1)}, u32[]{:S(2)}, u32[]{:S(2)}) collective-permute-start(bf16[448,256]{1,0:T(8,128)(2,1)S(1)} %fusion.18.gated), channel_id=1, source_target_pairs={{0,2},{2,4},{4,6},{6,8},{8,10},{10,12},{12,14},{14,16},{16,18},{18... | collective-permute-start | bytes 688136 | tf_op jit(solution)/shard_map/ppermute | solution.py:17
  9.8 12.2 %collective-permute-start = (bf16[64,256]{1,0:T(8,128)(2,1)S(1)}, bf16[64,256]{1,0:T(8,128)(2,1)S(1)}, u32[]{:S(2)}, u32[]{:S(2)}) collective-permute-start(bf16[64,256]{1,0:T(8,128)(2,1)S(1)} %slice.56), channel_id=1, source_target_pairs={{0,4},{2,6},{4,8},{6,10},{8,12},{10,14},{12,16},{14,18},{16,20},{1... | collective-permute-start | bytes 98312 | tf_op jit(solution)/shard_map/ppermute | solution.py:17
  21.9 0.6 copy-start.5
  21.9 0.7 %copy-start.3 = (bf16[448,256]{1,0:T(8,128)(2,1)}, bf16[448,256]{1,0:T(8,128)(2,1)S(1)}, u32[]{:S(2)}) copy-start(bf16[448,256]{1,0:T(8,128)(2,1)S(1)} %collective-permute-done.1.refs_14_) | copy-start | bytes 688132
  32.5 3.3 %copy-start.9 = (bf16[2,2048,256]{2,1,0:T(8,128)(2,1)S(1)}, bf16[2,2048,256]{2,1,0:T(8,128)(2,1)}, u32[]{:S(2)}) copy-start(bf16[2,2048,256]{2,1,0:T(8,128)(2,1)} %param.24) | copy-start | bytes 6291460
  35.8 1.2 %copy-start.12 = (bf16[448,2048]{1,0:T(8,128)(2,1)}, bf16[448,2048]{1,0:T(8,128)(2,1)S(1)}, u32[]{:S(2)}) copy-start(bf16[448,2048]{1,0:T(8,128)(2,1)S(1)} %get-tuple-element.48) | copy-start | bytes 5505028
  35.9 2.2 %copy-start.11 = (bf16[2,2048,256]{2,1,0:T(8,128)(2,1)S(1)}, bf16[2,2048,256]{2,1,0:T(8,128)(2,1)}, u32[]{:S(2)}) copy-start(bf16[2,2048,256]{2,1,0:T(8,128)(2,1)} %param.23) | copy-start | bytes 6291460
  38.8 3.9 %copy-start.2 = (bf16[448,256]{1,0:T(8,128)(2,1)}, bf16[448,256]{1,0:T(8,128)(2,1)S(1)}, u32[]{:S(2)}) copy-start(bf16[448,256]{1,0:T(8,128)(2,1)S(1)} %fusion.19.gated) | copy-start | bytes 688132
  38.8 11.1 %collective-permute-start.3 = (bf16[448,256]{1,0:T(8,128)(2,1)S(1)}, bf16[448,256]{1,0:T(8,128)(2,1)S(1)}, u32[]{:S(2)}, u32[]{:S(2)}) collective-permute-start(bf16[448,256]{1,0:T(8,128)(2,1)S(1)} %fusion.19.gated), channel_id=1, source_target_pairs={{0,2},{2,4},{4,6},{6,8},{8,10},{10,12},{12,14},{14,16},{16,18},{18... | collective-permute-start | bytes 688136 | tf_op jit(solution)/shard_map/ppermute | solution.py:17
  40.8 5.9 %collective-permute-start.2 = (bf16[64,256]{1,0:T(8,128)(2,1)S(1)}, bf16[64,256]{1,0:T(8,128)(2,1)S(1)}, u32[]{:S(2)}, u32[]{:S(2)}) collective-permute-start(bf16[64,256]{1,0:T(8,128)(2,1)S(1)} %slice.57), channel_id=1, source_target_pairs={{0,4},{2,6},{4,8},{6,10},{8,12},{10,14},{12,16},{14,18},{16,20},{1... | collective-permute-start | bytes 98312 | tf_op jit(solution)/shard_map/ppermute | solution.py:17
  46.7 3.2 %copy-start.6 = (bf16[64,256]{1,0:T(8,128)(2,1)}, bf16[64,256]{1,0:T(8,128)(2,1)S(1)}, u32[]{:S(2)}) copy-start(bf16[64,256]{1,0:T(8,128)(2,1)S(1)} %collective-permute-done.2.refs_13_) | copy-start | bytes 98308
  49.9 0.7 %copy-start.4 = (bf16[448,256]{1,0:T(8,128)(2,1)}, bf16[448,256]{1,0:T(8,128)(2,1)S(1)}, u32[]{:S(2)}) copy-start(bf16[448,256]{1,0:T(8,128)(2,1)S(1)} %collective-permute-done.3.refs_14_) | copy-start | bytes 688132
  50.6 10.4 %copy-start.13 = (bf16[448,2048]{1,0:T(8,128)(2,1)S(1)}, bf16[448,2048]{1,0:T(8,128)(2,1)}, u32[]{:S(2)}) copy-start(bf16[448,2048]{1,0:T(8,128)(2,1)} %copy-done.12) | copy-start | bytes 5505028

commit v2 on v1

v2 whole, which is shorter than its diff:
```python
import functools

import jax
import jax.numpy as jnp
import numpy as np
from jax import lax
from jax.experimental import pallas as pl
from jax.experimental.pallas import tpu as pltpu
from jax.sharding import PartitionSpec as P

STEP = 32
LIMIT = 20 << 20


def passed_along(value, axis, by):
    count = lax.axis_size(axis)
    pairs = [(i, (i + by) % count) for i in range(count) if by > 1 or i + by < count]
    return lax.ppermute(value, axis, pairs)


def scaled_rows(values, gain):
    scale = lax.rsqrt(jnp.mean(values * values, axis=-1, keepdims=True) + 1e-06)
    return (values * scale * gain).astype(jnp.bfloat16)


def gated_rows(normed, w_value, w_gate):
    values = dot(normed, w_value[...])
    gates = dot(normed, w_gate[...])
    return (values * jax.nn.sigmoid(gates)).astype(jnp.bfloat16)


def halves(rows):
    part = rows // 2 if rows % 32 == 0 else rows
    return [pl.ds(r, part) for r in range(0, rows, part)]


def first_gate_kernel(stream, gain, w_value, w_gate, gated, state, v_buf, g_buf, sems):
    pieces = halves(state.shape[0])
    copies = [pltpu.make_async_copy(stream.at[pieces[0]], state.at[pieces[0]], sems.at[0])]
    copies.append(pltpu.make_async_copy(w_value.at[0], v_buf, sems.at[1]))
    copies.append(pltpu.make_async_copy(w_gate.at[0], g_buf, sems.at[2]))
    for i, rows in enumerate(pieces[1:]):
        copies.append(pltpu.make_async_copy(stream.at[rows], state.at[rows], sems.at[3 + i]))
    for copy in copies:
        copy.start()
    copies[0].wait()
    normed = [scaled_rows(state[pieces[0], :].astype(jnp.float32), gain[0:1, :])]
    for copy in copies[1:]:
        copy.wait()
    for rows in pieces[1:]:
        normed.append(scaled_rows(state[rows, :].astype(jnp.float32), gain[0:1, :]))
    for rows, value in zip(pieces, normed):
        gated[rows, :] = gated_rows(value, v_buf, g_buf)


def mixed_rows(first, other, rows, here, gain, shift):
    own = first[rows, :].astype(jnp.float32)
    far = other[rows, :].astype(jnp.float32)
    values = jnp.concatenate([jnp.where(here == 0, own, far), jnp.where(here == 0, far, own)], axis=1)
    center = jnp.mean(values, axis=-1, keepdims=True)
    values = values - center
    spread = jnp.mean(jnp.square(values), axis=-1, keepdims=True)
    normed = values * lax.rsqrt(spread + 1e-05) * gain + shift
    return (normed * jax.nn.sigmoid(normed)).astype(jnp.bfloat16)


def mix_gate_kernel(
    here, own, far, ch_gain, ch_shift, w_out, state_h, gain, w_value, w_gate, new_state, gated, o_buf, v_buf, g_buf, state, sems, *, layer
):
    copies = [
        pltpu.make_async_copy(w_out.at[layer], o_buf, sems.at[0]),
        pltpu.make_async_copy(w_value.at[layer + 1], v_buf, sems.at[1]),
        pltpu.make_async_copy(w_gate.at[layer + 1], g_buf, sems.at[2]),
        pltpu.make_async_copy(state_h, state, sems.at[3]),
    ]
    for copy in copies:
        copy.start()
    pieces = halves(state.shape[0])
    at = slice(layer, layer + 1)
    mixed = [mixed_rows(own, far, rows, here[0], ch_gain[at, :], ch_shift[at, :]) for rows in pieces]
    copies[0].wait()
    copies[3].wait()
    for rows, value in zip(pieces, mixed):
        new_state[rows, :] = (state[rows, :].astype(jnp.float32) + dot(value, o_buf[...])).astype(jnp.bfloat16)
    copies[1].wait()
    copies[2].wait()
    for rows in pieces:
        normed = scaled_rows(new_state[rows, :].astype(jnp.float32), gain[layer + 1 : layer + 2, :])
        gated[rows, :] = gated_rows(normed, v_buf, g_buf)


def mix_kernel(here, own, far, ch_gain, ch_shift, w_out, state, out, o_buf, sems, *, layer):
    copy = pltpu.make_async_copy(w_out.at[layer], o_buf, sems.at[0])
    at = slice(layer, layer + 1)

    @pl.when(pl.program_id(0) == 0)
    def _():
        copy.start()

    rows = pl.ds(0, own.shape[0])
    mixed = mixed_rows(own, far, rows, here[0], ch_gain[at, :], ch_shift[at, :])

    @pl.when(pl.program_id(0) == 0)
    def _():
        copy.wait()

    out[...] = (state[...].astype(jnp.float32) + dot(mixed, o_buf[...])).astype(jnp.bfloat16)


def rotations(rows, cols, row_at, col_at, unit, scale):
    col = col_at(np.arange(cols, dtype=np.float64))
    coarse = row_at(np.arange(0, rows, STEP, dtype=np.float64))
    fine = row_at(np.arange(STEP, dtype=np.float64)) - row_at(np.float64(0))
    a = unit * np.outer(coarse, col)
    b = unit * np.outer(fine, col)
    both = [scale * np.cos(a), scale * np.sin(a), np.cos(b), np.sin(b)]
    return [x.astype(np.float32) for x in both]


def split(value, ref, rows, cols, apart):
    hi = value.astype(jnp.bfloat16)
    ref[rows, pl.ds(cols, value.shape[1])] = hi
    ref[rows, pl.ds(cols + apart, value.shape[1])] = (value - hi.astype(jnp.float32)).astype(jnp.bfloat16)


def dot(a, b):
    return jnp.dot(a, b, preferred_element_type=jnp.float32)


def parts(value):
    hi = value.astype(jnp.bfloat16)
    return hi, (value - hi.astype(jnp.float32)).astype(jnp.bfloat16)


def spread_rows(tables, i):
    ca, sa, cb, sb = tables
    c1 = ca[i : i + 1, :]
    s1 = sa[i : i + 1, :]
    c2 = cb[...]
    s2 = sb[...]
    return c1 * c2 - s1 * s2, s1 * c2 + c1 * s2


def forward_matrix(tables, out):
    half, span = out.shape[0] // 2, out.shape[1] // 2
    for i in range(tables[0].shape[0]):
        c, s = spread_rows(tables, i)
        split(c, out, pl.ds(i * STEP, STEP), 0, span)
        split(s, out, pl.ds(half + i * STEP, STEP), 0, span)


def prep_kernel(*refs):
    own_t, halo_t, back_t = refs[0:4], refs[4:8], refs[8:12]
    taps, own, halo, back, spectra = refs[12:17]
    forward_matrix(halo_t, halo)
    for layer in range(taps.shape[0]):
        t = taps[layer]
        spectra[layer] = dot(halo[...], jnp.concatenate([t, t], axis=0))
    forward_matrix(own_t, own)
    half = back.shape[1] // 4
    for i in range(back_t[0].shape[0]):
        c, s = spread_rows(back_t, i)
        rows = pl.ds(i * STEP, STEP)
        split(c, back, rows, 0, 2 * half)
        split(s, back, rows, half, 2 * half)


def own_kernel(matrix, gated, out):
    g = gated[...]
    missing = matrix.shape[1] // 2 - g.shape[0]
    if missing:
        g = jnp.concatenate([g, jnp.zeros((missing, g.shape[1]), g.dtype)], axis=0)
    out[...] = dot(matrix[...], jnp.concatenate([g, g], axis=0))


def finish_kernel(*refs, layer, pieces):
    halo, spectra, own, back, bias = refs[0:5]
    got = refs[5 : 5 + pieces]
    place, out = refs[5 + pieces : 7 + pieces]
    steps = range(pieces, 0, -1)
    window = [g[...] if n == 1 else jnp.where(place[0] < n, 0, g[...]).astype(jnp.bfloat16) for n, g in zip(steps, got)]
    far = dot(halo[...], jnp.concatenate(window * 2, axis=0))
    half = halo.shape[0] // 2
    w_c = own[:half, :] + far[:half]
    w_s = own[half:, :] + far[half:]
    h_c = spectra[layer, :half, :]
    h_s = spectra[layer, half:, :]
    re_hi, re_lo = parts(w_c * h_c + w_s * h_s)
    im_hi, im_lo = parts(w_s * h_c - w_c * h_s)
    y = dot(back[...], jnp.concatenate([re_hi, im_hi, re_hi, im_hi], axis=0))
    y += dot(back[:, : 2 * half], jnp.concatenate([re_lo, im_lo], axis=0))
    out[...] = (y + bias[layer : layer + 1, :]).astype(jnp.bfloat16)


def cost(flops, size):
    return pl.CostEstimate(flops=flops, bytes_accessed=size, transcendentals=0)


def per_device(
    stream,
    norm_gain,
    value_weight,
    gate_weight,
    conv_taps,
    conv_bias,
    channel_gain,
    channel_shift,
    out_weight,
):
    tokens = stream.shape[0]
    layers, width, chans = conv_taps.shape
    halo_rows = -(-(width - 1) // 128) * 128
    hops = -(-halo_rows // tokens)
    size = -(-(tokens + halo_rows) // 512) * 512
    half = size // 2
    unit = 2 * np.pi / size
    bf16, f32 = jnp.bfloat16, jnp.float32
    assert tokens % STEP == 0 and halo_rows >= width

    def freq(k):
        return k + 0.5

    span = -(-tokens // 128) * 128
    own_tab = rotations(half, span, freq, lambda t: t + 1, unit, 1.0)
    halo_tab = rotations(half, halo_rows, freq, lambda i: i + 1 - halo_rows, unit, 1.0)
    back_tab = rotations(tokens, half, lambda t: t + 1, freq, unit, 2.0 / size)
    taps = conv_taps
    if halo_rows > width:
        taps = jnp.pad(conv_taps, ((0, 0), (halo_rows - width, 0), (0, 0)))

    here = lax.axis_index("tp").astype(jnp.int32)[None]
    place = lax.axis_index("sp").astype(jnp.int32)[None]
    width_in = stream.shape[1]
    vmem, hbm, smem = (pl.BlockSpec(memory_space=m) for m in (pltpu.VMEM, pltpu.HBM, pltpu.SMEM))
    buf = pltpu.VMEM((width_in, chans), bf16)
    out_buf = pltpu.VMEM(out_weight.shape[1:], bf16)

    def held(*arrays):
        return [pltpu.with_memory_space_constraint(a, pltpu.VMEM) for a in arrays]

    def remote(*arrays):
        return [pltpu.with_memory_space_constraint(a, pltpu.HBM) for a in arrays]

    own_m, halo_m, back_m, spectra = pl.pallas_call(
        prep_kernel,
        out_shape=[
            jax.ShapeDtypeStruct((size, 2 * span), bf16),
            jax.ShapeDtypeStruct((size, 2 * halo_rows), bf16),
            jax.ShapeDtypeStruct((tokens, 2 * size), bf16),
            jax.ShapeDtypeStruct((layers, size, chans), f32),
        ],
        cost_estimate=cost(8 * layers * size * halo_rows * chans, 8 << 20),
        compiler_params=pltpu.CompilerParams(vmem_limit_bytes=LIMIT),
        name="prep",
    )(*own_tab, *halo_tab, *back_tab, taps)

    rows_buf = pltpu.VMEM((tokens, width_in), bf16)
    own_gated = pl.pallas_call(
        first_gate_kernel,
        in_specs=[hbm, vmem, hbm, hbm],
        out_shape=pltpu.VMEM((tokens, chans), bf16),
        out_specs=vmem,
        scratch_shapes=[rows_buf, buf, buf, pltpu.SemaphoreType.DMA((4,))],
        compiler_params=pltpu.CompilerParams(vmem_limit_bytes=LIMIT),
        name="first_gate",
    )(*remote(stream), norm_gain, *remote(value_weight, gate_weight))
    state = stream
    for layer in range(layers):
        pieces = []
        for step in range(1, hops + 1):
            count = min(tokens, halo_rows - (step - 1) * tokens)
            pieces.insert(0, passed_along(own_gated[tokens - count :], "sp", step))
        own_f = pl.pallas_call(
            own_kernel,
            in_specs=[vmem] * 2,
            out_shape=jax.ShapeDtypeStruct((size, chans), f32),
            cost_estimate=cost(8 * size * tokens * chans, 4 << 20),
            compiler_params=pltpu.CompilerParams(vmem_limit_bytes=LIMIT),
            name="own_part",
        )(own_m, own_gated)
        conv = pl.pallas_call(
            functools.partial(finish_kernel, layer=layer, pieces=len(pieces)),
            in_specs=[vmem] * (5 + len(pieces)) + [smem],
            out_shape=pltpu.VMEM((tokens, chans), bf16),
            out_specs=vmem,
            cost_estimate=cost(8 * size * halo_rows * chans, 4 << 20),
            compiler_params=pltpu.CompilerParams(vmem_limit_bytes=LIMIT),
            name="finish",
        )(halo_m, spectra, own_f, back_m, conv_bias, *pieces, place)
        far = lax.ppermute(conv, "tp", [(0, 1), (1, 0)])
        if layer + 1 < layers:
            state, own_gated = pl.pallas_call(
                functools.partial(mix_gate_kernel, layer=layer),
                in_specs=[smem, vmem, vmem, vmem, vmem, hbm, hbm, vmem, hbm, hbm],
                out_shape=[pltpu.VMEM((tokens, width_in), bf16), pltpu.VMEM((tokens, chans), bf16)],
                out_specs=[vmem, vmem],
                scratch_shapes=[out_buf, buf, buf, rows_buf, pltpu.SemaphoreType.DMA((4,))],
                compiler_params=pltpu.CompilerParams(vmem_limit_bytes=LIMIT),
                name="mix_gate",
            )(
                here,
                *held(conv, far),
                channel_gain,
                channel_shift,
                *remote(out_weight, state),
                norm_gain,
                *remote(value_weight, gate_weight),
            )
    steps = 4 if tokens % 64 == 0 else 1
    rows = tokens // steps

    def block(cols):
        return pl.BlockSpec((rows, cols), lambda i: (i, 0))

    def whole(array):
        return pl.BlockSpec(array.shape, lambda i: (0, 0))

    return pl.pallas_call(
        functools.partial(mix_kernel, layer=layers - 1),
        grid=(steps,),
        in_specs=[smem, block(chans), block(chans), whole(channel_gain), whole(channel_shift), hbm, block(width_in)],
        out_shape=jax.ShapeDtypeStruct((tokens, width_in), bf16),
        out_specs=block(width_in),
        scratch_shapes=[out_buf, pltpu.SemaphoreType.DMA((1,))],
        compiler_params=pltpu.CompilerParams(vmem_limit_bytes=LIMIT),
        name="mix",
    )(here, conv, far, channel_gain, channel_shift, *remote(out_weight), state)


def solution(mesh):
    return jax.shard_map(
        per_device,
        mesh=mesh,
        in_specs=(
            P("sp", None),
            P(),
            P(None, None, "tp"),
            P(None, None, "tp"),
            P(None, None, "tp"),
            P(None, "tp"),
            P(),
            P(),
            P(),
        ),
        out_specs=P("sp", None),
        check_vma=False,
    )
```

time: 65.7 us -> 52.2 us (0.79)
  matrix products: 12.3 us -> 0 us
  blocking collectives: 6.76 us -> 0 us
  waiting for transfers between devices: 4.01 us -> 9.89 us
  local copies, waits for them, and re-layouts: 4.1 us -> 7.11 us
  other arithmetic: 2.88 us -> 0 us
  Pallas kernels: 24.7 us -> 23.9 us
    dot_general x6 -> x0, matrix products: 12.3 us -> none  [the longest x2 7.52 us: per_device(): jnp.dot(mixed, out_weight[layer], preferred_element_type=jnp.float32)]
    all_gather x2 -> x0, blocking collectives: 6.76 us -> none  [per_device(): every_channel = lax.all_gather(conv, 'tp', axis=1, tiled=True)]
    pallas_call x2, Pallas kernels: 12.5 us -> 6.38 us  [per_device(): pl.pallas_call(functools.partial(finish_kernel, layer=layer, pieces=len(p...]
    pallas_call x3 -> x6, Pallas kernels: 12.1 us -> 17.5 us  [the longest x1 5.55 us: per_device(): pl.pallas_call(functools.partial(mix_gate_kernel, layer=layer), in_specs=...]
    unnamed x28 -> x50, local copies, waits for them, and re-layouts: 3.26 us -> 7.1 us
    ppermute x4, waiting for transfers between devices: 4.01 us -> 7.66 us  [passed_along(): return lax.ppermute(value, axis, pairs)]
    ppermute x0 -> x2, starting transfers between devices: none -> 3.63 us  [per_device(): far = lax.ppermute(conv, 'tp', [(0, 1), (1, 0)])]
    ppermute x4, starting transfers between devices: 10.2 us -> 7.05 us  [passed_along(): return lax.ppermute(value, axis, pairs)]
  transfers between devices with their start and end apart: 4 -> 6, of which waited for: 2 -> 5; matrix products, arithmetic and copies ran while one was open for 0% -> 0% of each run, Pallas kernels for 19% -> 7%
where the time goes in v2:
time: 52.2 us; the launch traced here: 51.8 us
  Pallas kernels  23.9 us (46%)
  starting transfers between devices  10.7 us (20%)
  waiting for transfers between devices  9.89 us (19%)
  local copies, waits for them, and re-layouts  7.11 us (14%)
    ppermute x4, waiting for transfers between devices, passed_along(): return lax.ppermute(value, axis, pairs)  7.66 us
    unnamed x50, local copies, waits for them, and re-layouts  7.1 us
    ppermute x4, starting transfers between devices, passed_along(): return lax.ppermute(value, axis, pairs)  7.05 us
    pallas_call x2, Pallas kernels, per_device(): pl.pallas_call(functools.partial(finish_kernel, layer=layer, pieces=len(p...  6.38 us
    pallas_call x1, Pallas kernels, per_device(): pl.pallas_call(functools.partial(mix_gate_kernel, layer=layer), in_specs=...  5.55 us
    pallas_call x1, Pallas kernels, per_device(): pl.pallas_call(functools.partial(mix_kernel, layer=layers - 1), grid=(ste...  5.03 us
    ppermute x2, starting transfers between devices, per_device(): far = lax.ppermute(conv, 'tp', [(0, 1), (1, 0)])  3.63 us
    pallas_call x1, Pallas kernels, per_device(): pl.pallas_call(first_gate_kernel, in_specs=[hbm, vmem, hbm, hbm], out_sha...  3.38 us
  transfers between devices with their start and end apart: 6, of which 5 were waited for; matrix products, arithmetic and copies ran while one was open for 0% of the time, Pallas kernels for 7%

profile of v2, /device:TPU:25, one launch (start us, length us, event | category | flops | bytes accessed | tf_op | source)
XLA Modules:
  0.0 51.8 jit_solution(17806167317198448232)
XLA Ops:
  0.0 0.0 copy-start.6
  0.0 0.7 %copy-done.6 = f32[2,2048]{1,0:T(2,128)S(1)} copy-done((f32[2,2048]{1,0:T(2,128)S(1)}, f32[2,2048]{1,0:T(2,128)}, u32[]{:S(2)}) %copy-start.6) | copy-done | bytes 16408
  0.7 0.0 copy-start.11
  0.7 0.0 copy-start.12
  0.7 0.0 copy-start.13
  0.7 0.0 copy-start.14
  0.7 0.0 copy-start.15
  0.7 0.0 copy-start.16
  0.8 0.0 copy-start.17
  0.8 0.0 copy-start.18
  0.8 0.0 copy-start.19
  0.8 0.0 copy-start.20
  0.8 0.0 copy-start.21
  0.8 0.0 copy-start.22
  0.8 3.4 %first_gate.1.gated = bf16[448,256]{1,0:T(8,128)(2,1)S(1)} custom-call(bf16[448,2048]{1,0:T(8,128)(2,1)} %state_h.1, f32[2,2048]{1,0:T(2,128)S(1)} %copy-done.6, bf16[2,2048,256]{2,1,0:T(8,128)(2,1)} %w_value.3, bf16[2,2048,256]{2,1,0:T(8,128)(2,1)} %w_gate.3), custom_call_target="tpu_custom_call" | custom-call | tf_op jit(solution)/shard_map/first_gate/pallas_call | solution.py:258
  4.2 3.1 %collective-permute-start.1 = (bf16[448,256]{1,0:T(8,128)(2,1)S(1)}, bf16[448,256]{1,0:T(8,128)(2,1)}, u32[]{:S(2)}, u32[]{:S(2)}) collective-permute-start(bf16[448,256]{1,0:T(8,128)(2,1)S(1)} %first_gate.1.gated), channel_id=1, source_target_pairs={{0,2},{2,4},{4,6},{6,8},{8,10},{10,12},{12,14},{14,16},{16,18},{18... | collective-permute-start | bytes 688136 | tf_op jit(solution)/shard_map/ppermute | solution.py:18
  7.4 1.3 %collective-permute-start = (bf16[64,256]{1,0:T(8,128)(2,1)S(1)}, bf16[64,256]{1,0:T(8,128)(2,1)S(1)}, u32[]{:S(2)}, u32[]{:S(2)}) collective-permute-start(bf16[64,256]{1,0:T(8,128)(2,1)S(1)} %slice.8), channel_id=1, source_target_pairs={{0,4},{2,6},{4,8},{6,10},{8,12},{10,14},{12,16},{14,18},{16,20},{1... | collective-permute-start | bytes 98312 | tf_op jit(solution)/shard_map/ppermute | solution.py:18
  8.7 0.0 copy-done.11
  8.7 0.0 copy-done.12
  8.7 0.0 copy-done.13
  8.7 0.0 copy-done.14
  8.7 0.0 copy-done.15
  8.7 0.0 copy-done.16
  8.7 0.0 copy-done.17
  8.7 0.0 copy-done.18
  8.7 0.0 copy-done.19
  8.7 0.0 copy-done.20
  8.7 0.0 copy-done.21
  8.7 0.0 copy-done.22
  8.8 2.1 %prep.1 = (bf16[1024,1024]{1,0:T(8,128)(2,1)S(1)}, bf16[1024,1024]{1,0:T(8,128)(2,1)S(1)}, bf16[448,2048]{1,0:T(8,128)(2,1)S(1)}, f32[2,1024,256]{2,1,0:T(8,128)S(1)}) custom-call(f32[16,512]{1,0:T(8,128)S(1)} %copy-done.22, f32[16,512]{1,0:T(8,128)S(1)} %copy-done.21, f32[32,512]{1,0:T(8,128)S(1)} %copy-done.17, f32[32,512]{1,0:T(8,128)S(1)} %copy-done.16, ...), custom_call_target="tpu_custom_call" | custom-call | flops 2147483648 | bytes 8388608 | tf_op jit(solution)/shard_map/prep/pallas_call | solution.py:244
  10.9 0.0 copy-start
  10.9 1.4 %copy-done = f32[2,1024,256]{2,1,0:T(8,128)} copy-done((f32[2,1024,256]{2,1,0:T(8,128)}, f32[2,1024,256]{2,1,0:T(8,128)S(1)}, u32[]{:S(2)}) %copy-start) | copy-done | bytes 2097176
  12.2 0.0 copy-start.3
  12.2 1.2 %copy-done.3 = bf16[448,2048]{1,0:T(8,128)(2,1)} copy-done((bf16[448,2048]{1,0:T(8,128)(2,1)}, bf16[448,2048]{1,0:T(8,128)(2,1)S(1)}, u32[]{:S(2)}) %copy-start.3) | copy-done | bytes 1835032
  13.5 0.0 copy-start.23
  13.5 0.0 copy-start.10
  13.5 0.7 %own_part.2.refs_2_ = f32[1024,256]{1,0:T(8,128)S(1)} custom-call(bf16[1024,1024]{1,0:T(8,128)(2,1)S(1)} %get-tuple-element.13.matrix, bf16[448,256]{1,0:T(8,128)(2,1)S(1)} %first_gate.1.gated), custom_call_target="tpu_custom_call" | custom-call | flops 939524096 | bytes 4194304 | tf_op jit(solution)/shard_map/own_part/pallas_call | solution.py:273
  14.2 0.6 %copy-done.23 = bf16[1024,1024]{1,0:T(8,128)(2,1)} copy-done((bf16[1024,1024]{1,0:T(8,128)(2,1)}, bf16[1024,1024]{1,0:T(8,128)(2,1)S(1)}, u32[]{:S(2)}) %copy-start.23) | copy-done | bytes 2097176
  14.8 0.0 collective-permute-done.refs_5_
  14.8 0.1 collective-permute-done.1.refs_6_
  14.9 0.0 copy-done.10
  14.9 1.6 %copy-done.1 = f32[2,1024,256]{2,1,0:T(8,128)S(1)} copy-done((f32[2,1024,256]{2,1,0:T(8,128)S(1)}, f32[2,1024,256]{2,1,0:T(8,128)}, u32[]{:S(2)}) %copy-start.1) | copy-done | bytes 2097176
  16.5 1.5 %copy-done.4 = bf16[448,2048]{1,0:T(8,128)(2,1)S(1)} copy-done((bf16[448,2048]{1,0:T(8,128)(2,1)S(1)}, bf16[448,2048]{1,0:T(8,128)(2,1)}, u32[]{:S(2)}) %copy-start.4) | copy-done | bytes 1835032
  18.0 3.6 %finish.2.own = bf16[448,256]{1,0:T(8,128)(2,1)S(1)} custom-call(bf16[1024,1024]{1,0:T(8,128)(2,1)S(1)} %get-tuple-element.11.refs_0_, f32[2,1024,256]{2,1,0:T(8,128)S(1)} %copy-done.1, f32[1024,256]{1,0:T(8,128)S(1)} %own_part.2.refs_2_, bf16[448,2048]{1,0:T(8,128)(2,1)S(1)} %copy-done.4, f32[2,256]{1,0:T(2,128)S(1)} %copy-done.10, ...), custom_call_target="tpu_custom_call" | custom-call | flops 1073741824 | bytes 4194304 | tf_op jit(solution)/shard_map/finish/pallas_call | solution.py:281
  21.7 2.0 %collective-permute-start.2 = (bf16[448,256]{1,0:T(8,128)(2,1)S(1)}, bf16[448,256]{1,0:T(8,128)(2,1)S(1)}, u32[]{:S(2)}, u32[]{:S(2)}) collective-permute-start(bf16[448,256]{1,0:T(8,128)(2,1)S(1)} %finish.2.own), channel_id=1, source_target_pairs={{0,1},{1,0},{2,3},{3,2},{4,5},{5,4},{6,7},{7,6},{8,9},{9,8},{10,11... | collective-permute-start | bytes 688136 | tf_op jit(solution)/shard_map/ppermute | solution.py:290
  23.7 1.1 %collective-permute-done.2.far = bf16[448,256]{1,0:T(8,128)(2,1)S(1)} collective-permute-done((bf16[448,256]{1,0:T(8,128)(2,1)S(1)}, bf16[448,256]{1,0:T(8,128)(2,1)S(1)}, u32[]{:S(2)}, u32[]{:S(2)}) %collective-permute-start.2) | collective-permute-done | bytes 229408 | tf_op jit(solution)/shard_map/ppermute | solution.py:290
  24.8 0.0 copy-done.7
  24.8 0.0 copy-done.8
  24.8 0.0 copy-done.9
  24.8 0.0 copy-start.5
  24.8 5.5 %mix_gate.1 = (bf16[448,2048]{1,0:T(8,128)(2,1)S(1)}, bf16[448,256]{1,0:T(8,128)(2,1)S(1)}) custom-call(s32[1]{0:T(128)} %bitcast.here, bf16[448,256]{1,0:T(8,128)(2,1)S(1)} %finish.2.own, bf16[448,256]{1,0:T(8,128)(2,1)S(1)} %collective-permute-done.2.far, f32[2,512]{1,0:T(2,128)S(1)} %copy-done.8, f32[2,512]{1,0:T(2,128)S(1)} %copy-done.9, ...), custom_call_target="tpu_custom_call" | custom-call | tf_op jit(solution)/shard_map/mix_gate/pallas_call | solution.py:292
  30.3 0.0 copy-start.2
  30.4 2.6 %collective-permute-start.4 = (bf16[448,256]{1,0:T(8,128)(2,1)S(1)}, bf16[448,256]{1,0:T(8,128)(2,1)S(1)}, u32[]{:S(2)}, u32[]{:S(2)}) collective-permute-start(bf16[448,256]{1,0:T(8,128)(2,1)S(1)} %get-tuple-element.15.gated), channel_id=1, source_target_pairs={{0,2},{2,4},{4,6},{6,8},{8,10},{10,12},{12,14},{14,16},{16,18},{18... | collective-permute-start | bytes 688136 | tf_op jit(solution)/shard_map/ppermute | solution.py:18
  33.0 0.1 collective-permute-start.3
  33.0 0.0 copy-done.24
  33.0 0.7 %own_part.3.refs_2_ = f32[1024,256]{1,0:T(8,128)S(1)} custom-call(bf16[1024,1024]{1,0:T(8,128)(2,1)S(1)} %copy-done.24, bf16[448,256]{1,0:T(8,128)(2,1)S(1)} %get-tuple-element.15.gated), custom_call_target="tpu_custom_call" | custom-call | flops 939524096 | bytes 4194304 | tf_op jit(solution)/shard_map/own_part/pallas_call | solution.py:273
  33.8 3.0 %collective-permute-done.3.refs_5_ = bf16[64,256]{1,0:T(8,128)(2,1)S(1)} collective-permute-done((bf16[64,256]{1,0:T(8,128)(2,1)S(1)}, bf16[64,256]{1,0:T(8,128)(2,1)S(1)}, u32[]{:S(2)}, u32[]{:S(2)}) %collective-permute-start.3) | collective-permute-done | bytes 32800 | tf_op jit(solution)/shard_map/ppermute | solution.py:18
  36.7 4.5 %collective-permute-done.4.refs_6_ = bf16[448,256]{1,0:T(8,128)(2,1)S(1)} collective-permute-done((bf16[448,256]{1,0:T(8,128)(2,1)S(1)}, bf16[448,256]{1,0:T(8,128)(2,1)S(1)}, u32[]{:S(2)}, u32[]{:S(2)}) %collective-permute-start.4) | collective-permute-done | bytes 229408 | tf_op jit(solution)/shard_map/ppermute | solution.py:18
  41.3 0.0 copy-done.5
  41.3 0.0 copy-done.2
  41.3 2.7 %finish.3.own = bf16[448,256]{1,0:T(8,128)(2,1)S(1)} custom-call(bf16[1024,1024]{1,0:T(8,128)(2,1)S(1)} %get-tuple-element.11.refs_0_, f32[2,1024,256]{2,1,0:T(8,128)S(1)} %copy-done.2, f32[1024,256]{1,0:T(8,128)S(1)} %own_part.3.refs_2_, bf16[448,2048]{1,0:T(8,128)(2,1)S(1)} %copy-done.5, f32[2,256]{1,0:T(2,128)S(1)} %copy-done.10, ...), custom_call_target="tpu_custom_call" | custom-call | flops 1073741824 | bytes 4194304 | tf_op jit(solution)/shard_map/finish/pallas_call | solution.py:281
  44.0 1.7 %collective-permute-start.5 = (bf16[448,256]{1,0:T(8,128)(2,1)S(1)}, bf16[448,256]{1,0:T(8,128)(2,1)S(1)}, u32[]{:S(2)}, u32[]{:S(2)}) collective-permute-start(bf16[448,256]{1,0:T(8,128)(2,1)S(1)} %finish.3.own), channel_id=1, source_target_pairs={{0,1},{1,0},{2,3},{3,2},{4,5},{5,4},{6,7},{7,6},{8,9},{9,8},{10,11... | collective-permute-start | bytes 688136 | tf_op jit(solution)/shard_map/ppermute | solution.py:290
  45.7 1.1 %collective-permute-done.5.far = bf16[448,256]{1,0:T(8,128)(2,1)S(1)} collective-permute-done((bf16[448,256]{1,0:T(8,128)(2,1)S(1)}, bf16[448,256]{1,0:T(8,128)(2,1)S(1)}, u32[]{:S(2)}, u32[]{:S(2)}) %collective-permute-start.5) | collective-permute-done | bytes 229408 | tf_op jit(solution)/shard_map/ppermute | solution.py:290
  46.8 5.0 %mix.1 = bf16[448,2048]{1,0:T(8,128)(2,1)} custom-call(s32[1]{0:T(128)} %bitcast.here, bf16[448,256]{1,0:T(8,128)(2,1)S(1)} %finish.3.own, bf16[448,256]{1,0:T(8,128)(2,1)S(1)} %collective-permute-done.5.far, f32[2,512]{1,0:T(2,128)S(1)} %copy-done.8, f32[2,512]{1,0:T(2,128)S(1)} %copy-done.9, bf16[2,512,2048]{2,1,0:T(8,128)(2,1)} %w_out.3, ...), custom_call_target="tpu_custom_call" | custom-call | tf_op jit(solution)/shard_map/mix/pallas_call | solution.py:318
  (8 shorter events, 0.0 us)
Async XLA Ops:
  0.0 0.7 %copy-start.6 = (f32[2,2048]{1,0:T(2,128)S(1)}, f32[2,2048]{1,0:T(2,128)}, u32[]{:S(2)}) copy-start(f32[2,2048]{1,0:T(2,128)} %gain.3) | copy-start | bytes 49156
  0.7 7.9 %copy-start.11 = (bf16[2,512,256]{2,1,0:T(8,128)(2,1)S(1)}, bf16[2,512,256]{2,1,0:T(8,128)(2,1)}, u32[]{:S(2)}) copy-start(bf16[2,512,256]{2,1,0:T(8,128)(2,1)} %refs_12_.1) | copy-start | bytes 1572868
  0.7 7.9 %copy-start.12 = (f32[32,512]{1,0:T(8,128)S(1)}, f32[32,512]{1,0:T(8,128)}, u32[]{:S(2)}) copy-start(f32[32,512]{1,0:T(8,128)} %constant.40.clone.refs_11_) | copy-start | bytes 196612
  0.7 7.9 %copy-start.13 = (f32[32,512]{1,0:T(8,128)S(1)}, f32[32,512]{1,0:T(8,128)}, u32[]{:S(2)}) copy-start(f32[32,512]{1,0:T(8,128)} %constant.39.clone.refs_10_) | copy-start | bytes 196612
  0.7 7.9 %copy-start.14 = (f32[32,512]{1,0:T(8,128)S(1)}, f32[32,512]{1,0:T(8,128)}, u32[]{:S(2)}) copy-start(f32[32,512]{1,0:T(8,128)} %constant.36.clone.refs_7_) | copy-start | bytes 196612
  0.7 7.9 %copy-start.15 = (f32[32,512]{1,0:T(8,128)S(1)}, f32[32,512]{1,0:T(8,128)}, u32[]{:S(2)}) copy-start(f32[32,512]{1,0:T(8,128)} %constant.35.clone.refs_6_) | copy-start | bytes 196612
  0.7 7.9 %copy-start.16 = (f32[32,512]{1,0:T(8,128)S(1)}, f32[32,512]{1,0:T(8,128)}, u32[]{:S(2)}) copy-start(f32[32,512]{1,0:T(8,128)} %constant.33.clone.refs_3_) | copy-start | bytes 196612
  0.8 7.9 %copy-start.17 = (f32[32,512]{1,0:T(8,128)S(1)}, f32[32,512]{1,0:T(8,128)}, u32[]{:S(2)}) copy-start(f32[32,512]{1,0:T(8,128)} %constant.32.clone.refs_2_) | copy-start | bytes 196612
  0.8 7.9 %copy-start.18 = (f32[14,512]{1,0:T(8,128)S(1)}, f32[14,512]{1,0:T(8,128)}, u32[]{:S(2)}) copy-start(f32[14,512]{1,0:T(8,128)} %constant.38.clone.refs_9_) | copy-start | bytes 86020
  0.8 7.9 %copy-start.19 = (f32[14,512]{1,0:T(8,128)S(1)}, f32[14,512]{1,0:T(8,128)}, u32[]{:S(2)}) copy-start(f32[14,512]{1,0:T(8,128)} %constant.37.clone.refs_8_) | copy-start | bytes 86020
  0.8 7.9 %copy-start.20 = (f32[16,512]{1,0:T(8,128)S(1)}, f32[16,512]{1,0:T(8,128)}, u32[]{:S(2)}) copy-start(f32[16,512]{1,0:T(8,128)} %constant.34.clone.refs_5_) | copy-start | bytes 98308
  0.8 7.9 %copy-start.21 = (f32[16,512]{1,0:T(8,128)S(1)}, f32[16,512]{1,0:T(8,128)}, u32[]{:S(2)}) copy-start(f32[16,512]{1,0:T(8,128)} %constant.31.clone.refs_1_.refs_4_) | copy-start | bytes 98308
  0.8 7.9 %copy-start.22 = (f32[16,512]{1,0:T(8,128)S(1)}, f32[16,512]{1,0:T(8,128)}, u32[]{:S(2)}) copy-start(f32[16,512]{1,0:T(8,128)} %constant.30.clone.refs_0_) | copy-start | bytes 98308
  4.2 10.7 %collective-permute-start.1 = (bf16[448,256]{1,0:T(8,128)(2,1)S(1)}, bf16[448,256]{1,0:T(8,128)(2,1)}, u32[]{:S(2)}, u32[]{:S(2)}) collective-permute-start(bf16[448,256]{1,0:T(8,128)(2,1)S(1)} %first_gate.1.gated), channel_id=1, source_target_pairs={{0,2},{2,4},{4,6},{6,8},{8,10},{10,12},{12,14},{14,16},{16,18},{18... | collective-permute-start | bytes 688136 | tf_op jit(solution)/shard_map/ppermute | solution.py:18
  7.4 7.4 %collective-permute-start = (bf16[64,256]{1,0:T(8,128)(2,1)S(1)}, bf16[64,256]{1,0:T(8,128)(2,1)S(1)}, u32[]{:S(2)}, u32[]{:S(2)}) collective-permute-start(bf16[64,256]{1,0:T(8,128)(2,1)S(1)} %slice.8), channel_id=1, source_target_pairs={{0,4},{2,6},{4,8},{6,10},{8,12},{10,14},{12,16},{14,18},{16,20},{1... | collective-permute-start | bytes 98312 | tf_op jit(solution)/shard_map/ppermute | solution.py:18
  10.9 1.4 %copy-start = (f32[2,1024,256]{2,1,0:T(8,128)}, f32[2,1024,256]{2,1,0:T(8,128)S(1)}, u32[]{:S(2)}) copy-start(f32[2,1024,256]{2,1,0:T(8,128)S(1)} %get-tuple-element.12.refs_1_) | copy-start | bytes 6291460
  12.2 1.2 %copy-start.3 = (bf16[448,2048]{1,0:T(8,128)(2,1)}, bf16[448,2048]{1,0:T(8,128)(2,1)S(1)}, u32[]{:S(2)}) copy-start(bf16[448,2048]{1,0:T(8,128)(2,1)S(1)} %get-tuple-element.14.refs_3_) | copy-start | bytes 5505028
  13.5 1.3 %copy-start.23 = (bf16[1024,1024]{1,0:T(8,128)(2,1)}, bf16[1024,1024]{1,0:T(8,128)(2,1)S(1)}, u32[]{:S(2)}) copy-start(bf16[1024,1024]{1,0:T(8,128)(2,1)S(1)} %get-tuple-element.13.matrix) | copy-start | bytes 6291460
  13.5 1.5 %copy-start.10 = (f32[2,256]{1,0:T(2,128)S(1)}, f32[2,256]{1,0:T(2,128)}, u32[]{:S(2)}) copy-start(f32[2,256]{1,0:T(2,128)} %refs_4_.4) | copy-start | bytes 6148
  14.9 1.6 %copy-start.1 = (f32[2,1024,256]{2,1,0:T(8,128)S(1)}, f32[2,1024,256]{2,1,0:T(8,128)}, u32[]{:S(2)}) copy-start(f32[2,1024,256]{2,1,0:T(8,128)} %copy-done) | copy-start | bytes 6291460
  16.5 1.5 %copy-start.4 = (bf16[448,2048]{1,0:T(8,128)(2,1)S(1)}, bf16[448,2048]{1,0:T(8,128)(2,1)}, u32[]{:S(2)}) copy-start(bf16[448,2048]{1,0:T(8,128)(2,1)} %copy-done.3) | copy-start | bytes 5505028
  18.0 6.7 %copy-start.7 = (f32[2,2048]{1,0:T(2,128)S(1)}, f32[2,2048]{1,0:T(2,128)}, u32[]{:S(2)}) copy-start(f32[2,2048]{1,0:T(2,128)} %gain.3) | copy-start | bytes 49156
  18.0 6.7 %copy-start.8 = (f32[2,512]{1,0:T(2,128)S(1)}, f32[2,512]{1,0:T(2,128)}, u32[]{:S(2)}) copy-start(f32[2,512]{1,0:T(2,128)} %ch_gain.3) | copy-start | bytes 12292
  18.0 6.7 %copy-start.9 = (f32[2,512]{1,0:T(2,128)S(1)}, f32[2,512]{1,0:T(2,128)}, u32[]{:S(2)}) copy-start(f32[2,512]{1,0:T(2,128)} %ch_shift.3) | copy-start | bytes 12292
  21.7 3.1 %collective-permute-start.2 = (bf16[448,256]{1,0:T(8,128)(2,1)S(1)}, bf16[448,256]{1,0:T(8,128)(2,1)S(1)}, u32[]{:S(2)}, u32[]{:S(2)}) collective-permute-start(bf16[448,256]{1,0:T(8,128)(2,1)S(1)} %finish.2.own), channel_id=1, source_target_pairs={{0,1},{1,0},{2,3},{3,2},{4,5},{5,4},{6,7},{7,6},{8,9},{9,8},{10,11... | collective-permute-start | bytes 688136 | tf_op jit(solution)/shard_map/ppermute | solution.py:290
  24.8 8.2 %copy-start.24 = (bf16[1024,1024]{1,0:T(8,128)(2,1)S(1)}, bf16[1024,1024]{1,0:T(8,128)(2,1)}, u32[]{:S(2)}) copy-start(bf16[1024,1024]{1,0:T(8,128)(2,1)} %copy-done.23) | copy-start | bytes 6291460
  24.8 16.5 %copy-start.5 = (bf16[448,2048]{1,0:T(8,128)(2,1)S(1)}, bf16[448,2048]{1,0:T(8,128)(2,1)}, u32[]{:S(2)}) copy-start(bf16[448,2048]{1,0:T(8,128)(2,1)} %copy-done.3) | copy-start | bytes 5505028
  30.3 10.9 %copy-start.2 = (f32[2,1024,256]{2,1,0:T(8,128)S(1)}, f32[2,1024,256]{2,1,0:T(8,128)}, u32[]{:S(2)}) copy-start(f32[2,1024,256]{2,1,0:T(8,128)} %copy-done) | copy-start | bytes 6291460
  30.4 10.9 %collective-permute-start.4 = (bf16[448,256]{1,0:T(8,128)(2,1)S(1)}, bf16[448,256]{1,0:T(8,128)(2,1)S(1)}, u32[]{:S(2)}, u32[]{:S(2)}) collective-permute-start(bf16[448,256]{1,0:T(8,128)(2,1)S(1)} %get-tuple-element.15.gated), channel_id=1, source_target_pairs={{0,2},{2,4},{4,6},{6,8},{8,10},{10,12},{12,14},{14,16},{16,18},{18... | collective-permute-start | bytes 688136 | tf_op jit(solution)/shard_map/ppermute | solution.py:18
  33.0 3.8 %collective-permute-start.3 = (bf16[64,256]{1,0:T(8,128)(2,1)S(1)}, bf16[64,256]{1,0:T(8,128)(2,1)S(1)}, u32[]{:S(2)}, u32[]{:S(2)}) collective-permute-start(bf16[64,256]{1,0:T(8,128)(2,1)S(1)} %slice.7), channel_id=1, source_target_pairs={{0,4},{2,6},{4,8},{6,10},{8,12},{10,14},{12,16},{14,18},{16,20},{1... | collective-permute-start | bytes 98312 | tf_op jit(solution)/shard_map/ppermute | solution.py:18
  44.0 2.8 %collective-permute-start.5 = (bf16[448,256]{1,0:T(8,128)(2,1)S(1)}, bf16[448,256]{1,0:T(8,128)(2,1)S(1)}, u32[]{:S(2)}, u32[]{:S(2)}) collective-permute-start(bf16[448,256]{1,0:T(8,128)(2,1)S(1)} %finish.3.own), channel_id=1, source_target_pairs={{0,1},{1,0},{2,3},{3,2},{4,5},{5,4},{6,7},{7,6},{8,9},{9,8},{10,11... | collective-permute-start | bytes 688136 | tf_op jit(solution)/shard_map/ppermute | solution.py:290

commit v3 on v2

v3 whole, which is shorter than its diff:
```python
import functools

import jax
import jax.numpy as jnp
import numpy as np
from jax import lax
from jax.experimental import pallas as pl
from jax.experimental.pallas import tpu as pltpu
from jax.sharding import PartitionSpec as P

STEP = 32
LIMIT = 20 << 20


def passed_along(value, axis, by):
    count = lax.axis_size(axis)
    pairs = [(i, (i + by) % count) for i in range(count) if by > 1 or i + by < count]
    return lax.ppermute(value, axis, pairs)


def chunks(total, part):
    part = part if total % part == 0 else total
    return [pl.ds(r, part) for r in range(0, total, part)]


def gate_all(normed, w_value, w_gate, gated, tail):
    values = dot(normed[...], w_value[...])
    gates = dot(normed[...], w_gate[...])
    out = (values * jax.nn.sigmoid(gates)).astype(jnp.bfloat16)
    gated[...] = out
    tail[...] = out[out.shape[0] - tail.shape[0] :]


def first_gate_kernel(stream, gain_h, w_value, w_gate, tail, gated, state, normed, gain, v_buf, g_buf, sems):
    total = state.shape[0]
    pieces = chunks(total, 64)
    copies = [pltpu.make_async_copy(gain_h, gain, sems.at[0])]
    for i, rows in enumerate(pieces):
        copies.append(pltpu.make_async_copy(stream.at[rows], state.at[rows], sems.at[3 + i]))
    copies.append(pltpu.make_async_copy(w_value.at[0], v_buf, sems.at[1]))
    copies.append(pltpu.make_async_copy(w_gate.at[0], g_buf, sems.at[2]))
    for copy in copies:
        copy.start()
    copies[0].wait()
    for i, piece in enumerate(pieces):
        copies[1 + i].wait()
        for part in chunks(piece.size, 32):
            rows = pl.ds(piece.start + part.start, part.size)
            values = state[rows, :].astype(jnp.float32)
            scale = lax.rsqrt(jnp.mean(values * values, axis=-1, keepdims=True) + 1e-06)
            normed[rows, :] = (values * scale * gain[0:1, :]).astype(jnp.bfloat16)
    copies[-2].wait()
    copies[-1].wait()
    gate_all(normed, v_buf, g_buf, gated, tail)


def mix_all(first, other, gain, shift, mixed):
    here = lax.axis_index("tp")
    for rows in chunks(mixed.shape[0], 64):
        own = first[rows, :].astype(jnp.float32)
        far = other[rows, :].astype(jnp.float32)
        values = jnp.concatenate([jnp.where(here == 0, own, far), jnp.where(here == 0, far, own)], axis=1)
        center = jnp.mean(values, axis=-1, keepdims=True)
        values = values - center
        spread = jnp.mean(jnp.square(values), axis=-1, keepdims=True)
        normed = values * lax.rsqrt(spread + 1e-05) * gain + shift
        mixed[rows, :] = (normed * jax.nn.sigmoid(normed)).astype(jnp.bfloat16)


def mix_gate_kernel(
    own, far, ch_gain, ch_shift, w_out, state, gain, w_value, w_gate,
    new_state, gated, tail, mixed, normed, v_buf, g_buf, sems, *, layer
):
    copies = [
        pltpu.make_async_copy(w_value.at[layer + 1], v_buf, sems.at[0]),
        pltpu.make_async_copy(w_gate.at[layer + 1], g_buf, sems.at[1]),
    ]
    for copy in copies:
        copy.start()
    at = slice(layer, layer + 1)
    mix_all(own, far, ch_gain[at, :], ch_shift[at, :], mixed)
    width = new_state.shape[1]
    total = 0.0
    for cols in chunks(width, 512):
        update = dot(mixed[...], w_out[layer, :, cols])
        new = (state[:, cols].astype(jnp.float32) + update).astype(jnp.bfloat16)
        new_state[:, cols] = new
        new = new.astype(jnp.float32)
        total += jnp.sum(new * new, axis=-1, keepdims=True)
    scale = lax.rsqrt(total / width + 1e-06)
    for cols in chunks(width, 512):
        values = new_state[:, cols].astype(jnp.float32)
        normed[:, cols] = (values * scale * gain[layer + 1 : layer + 2, cols]).astype(jnp.bfloat16)
    for copy in copies:
        copy.wait()
    gate_all(normed, v_buf, g_buf, gated, tail)


def mix_kernel(own, far, ch_gain, ch_shift, w_out, state, out_h, mixed, out, sems, *, layer):
    at = slice(layer, layer + 1)
    mix_all(own, far, ch_gain[at, :], ch_shift[at, :], mixed)
    copies = []
    for i, cols in enumerate(chunks(state.shape[1], 512)):
        update = dot(mixed[...], w_out[layer, :, cols])
        out[:, cols] = (state[:, cols].astype(jnp.float32) + update).astype(jnp.bfloat16)
        copies.append(pltpu.make_async_copy(out.at[:, cols], out_h.at[:, cols], sems.at[i]))
        copies[-1].start()
    for copy in copies:
        copy.wait()


def rotations(rows, cols, row_at, col_at, unit, scale):
    col = col_at(np.arange(cols, dtype=np.float64))
    coarse = row_at(np.arange(0, rows, STEP, dtype=np.float64))
    fine = row_at(np.arange(STEP, dtype=np.float64)) - row_at(np.float64(0))
    a = unit * np.outer(coarse, col)
    b = unit * np.outer(fine, col)
    both = [scale * np.cos(a), scale * np.sin(a), np.cos(b), np.sin(b)]
    return [x.astype(np.float32) for x in both]


def split(value, ref, rows, cols, apart):
    hi = value.astype(jnp.bfloat16)
    ref[rows, pl.ds(cols, value.shape[1])] = hi
    ref[rows, pl.ds(cols + apart, value.shape[1])] = (value - hi.astype(jnp.float32)).astype(jnp.bfloat16)


def dot(a, b):
    return jnp.dot(a, b, preferred_element_type=jnp.float32)


def parts(value):
    hi = value.astype(jnp.bfloat16)
    return hi, (value - hi.astype(jnp.float32)).astype(jnp.bfloat16)


def spread_rows(tables, i):
    ca, sa, cb, sb = tables
    c1 = ca[i : i + 1, :]
    s1 = sa[i : i + 1, :]
    c2 = cb[...]
    s2 = sb[...]
    return c1 * c2 - s1 * s2, s1 * c2 + c1 * s2


def forward_matrix(tables, out):
    half, span = out.shape[0] // 2, out.shape[1] // 2
    for i in range(tables[0].shape[0]):
        c, s = spread_rows(tables, i)
        split(c, out, pl.ds(i * STEP, STEP), 0, span)
        split(s, out, pl.ds(half + i * STEP, STEP), 0, span)


def prep_kernel(*refs):
    own_t, halo_t, back_t = refs[0:4], refs[4:8], refs[8:12]
    taps, own, halo, back, spectra = refs[12:17]
    forward_matrix(halo_t, halo)
    for layer in range(taps.shape[0]):
        t = taps[layer]
        spectra[layer] = dot(halo[...], jnp.concatenate([t, t], axis=0))
    forward_matrix(own_t, own)
    half = back.shape[1] // 4
    for i in range(back_t[0].shape[0]):
        c, s = spread_rows(back_t, i)
        rows = pl.ds(i * STEP, STEP)
        split(c, back, rows, 0, 2 * half)
        split(s, back, rows, half, 2 * half)


def own_kernel(matrix, gated, out):
    g = gated[...]
    missing = matrix.shape[1] // 2 - g.shape[0]
    if missing:
        g = jnp.concatenate([g, jnp.zeros((missing, g.shape[1]), g.dtype)], axis=0)
    out[...] = dot(matrix[...], jnp.concatenate([g, g], axis=0))


def finish_kernel(*refs, layer, pieces):
    halo, spectra, own, back, bias = refs[0:5]
    got = refs[5 : 5 + pieces]
    out = refs[5 + pieces]
    place = lax.axis_index("sp")
    steps = range(pieces, 0, -1)
    window = [g[...] if n == 1 else jnp.where(place < n, 0, g[...]).astype(jnp.bfloat16) for n, g in zip(steps, got)]
    far = dot(halo[...], jnp.concatenate(window * 2, axis=0))
    half = halo.shape[0] // 2
    w_c = own[:half, :] + far[:half]
    w_s = own[half:, :] + far[half:]
    h_c = spectra[layer, :half, :]
    h_s = spectra[layer, half:, :]
    re_hi, re_lo = parts(w_c * h_c + w_s * h_s)
    im_hi, im_lo = parts(w_s * h_c - w_c * h_s)
    y = dot(back[...], jnp.concatenate([re_hi, im_hi, re_hi, im_hi], axis=0))
    y += dot(back[:, : 2 * half], jnp.concatenate([re_lo, im_lo], axis=0))
    out[...] = (y + bias[layer : layer + 1, :]).astype(jnp.bfloat16)


def cost(flops, size):
    return pl.CostEstimate(flops=flops, bytes_accessed=size, transcendentals=0)


def per_device(
    stream,
    norm_gain,
    value_weight,
    gate_weight,
    conv_taps,
    conv_bias,
    channel_gain,
    channel_shift,
    out_weight,
):
    tokens = stream.shape[0]
    layers, width, chans = conv_taps.shape
    halo_rows = -(-(width - 1) // 128) * 128
    hops = -(-halo_rows // tokens)
    size = -(-(tokens + halo_rows) // 512) * 512
    half = size // 2
    unit = 2 * np.pi / size
    bf16, f32 = jnp.bfloat16, jnp.float32
    assert tokens % STEP == 0 and halo_rows >= width

    def freq(k):
        return k + 0.5

    span = -(-tokens // 128) * 128
    own_tab = rotations(half, span, freq, lambda t: t + 1, unit, 1.0)
    halo_tab = rotations(half, halo_rows, freq, lambda i: i + 1 - halo_rows, unit, 1.0)
    back_tab = rotations(tokens, half, lambda t: t + 1, freq, unit, 2.0 / size)
    taps = conv_taps
    if halo_rows > width:
        taps = jnp.pad(conv_taps, ((0, 0), (halo_rows - width, 0), (0, 0)))

    width_in = stream.shape[1]
    vmem, hbm = (pl.BlockSpec(memory_space=m) for m in (pltpu.VMEM, pltpu.HBM))
    buf = pltpu.VMEM((width_in, chans), bf16)
    last = halo_rows - (hops - 1) * tokens
    columns = len(chunks(width_in, 512))
    params = pltpu.CompilerParams(vmem_limit_bytes=LIMIT)

    def remote(*arrays):
        return [pltpu.with_memory_space_constraint(a, pltpu.HBM) for a in arrays]

    own_m, halo_m, back_m, spectra = pl.pallas_call(
        prep_kernel,
        out_shape=[
            jax.ShapeDtypeStruct((size, 2 * span), bf16),
            jax.ShapeDtypeStruct((size, 2 * halo_rows), bf16),
            jax.ShapeDtypeStruct((tokens, 2 * size), bf16),
            jax.ShapeDtypeStruct((layers, size, chans), f32),
        ],
        cost_estimate=cost(8 * layers * size * halo_rows * chans, 8 << 20),
        compiler_params=pltpu.CompilerParams(vmem_limit_bytes=LIMIT),
        name="prep",
    )(*own_tab, *halo_tab, *back_tab, taps)

    rows_buf = pltpu.VMEM((tokens, width_in), bf16)
    mixed_buf = pltpu.VMEM((tokens, out_weight.shape[1]), bf16)
    gated_out = [pltpu.VMEM((tokens, chans), bf16), pltpu.VMEM((last, chans), bf16)]
    tail, own_gated = pl.pallas_call(
        first_gate_kernel,
        in_specs=[hbm] * 4,
        out_shape=gated_out[::-1],
        out_specs=[vmem] * 2,
        scratch_shapes=[
            rows_buf,
            rows_buf,
            pltpu.VMEM(norm_gain.shape, f32),
            buf,
            buf,
            pltpu.SemaphoreType.DMA((3 + len(chunks(tokens, 64)),)),
        ],
        compiler_params=params,
        name="first_gate",
    )(*remote(stream, norm_gain, value_weight, gate_weight))
    state = stream
    for layer in range(layers):
        pieces = []
        for step in range(hops, 0, -1):
            pieces.append(passed_along(own_gated if step < hops else tail, "sp", step))
        own_f = pl.pallas_call(
            own_kernel,
            in_specs=[vmem] * 2,
            out_shape=jax.ShapeDtypeStruct((size, chans), f32),
            cost_estimate=cost(8 * size * tokens * chans, 4 << 20),
            compiler_params=params,
            name="own_part",
        )(own_m, own_gated)
        conv = pl.pallas_call(
            functools.partial(finish_kernel, layer=layer, pieces=len(pieces)),
            in_specs=[vmem] * (5 + len(pieces)),
            out_shape=pltpu.VMEM((tokens, chans), bf16),
            out_specs=vmem,
            cost_estimate=cost(8 * size * halo_rows * chans, 4 << 20),
            compiler_params=params,
            name="finish",
        )(halo_m, spectra, own_f, back_m, conv_bias, *pieces)
        far = lax.ppermute(conv, "tp", [(0, 1), (1, 0)])
        if layer + 1 < layers:
            state, own_gated, tail = pl.pallas_call(
                functools.partial(mix_gate_kernel, layer=layer),
                in_specs=[vmem] * 7 + [hbm] * 2,
                out_shape=[pltpu.VMEM((tokens, width_in), bf16)] + gated_out,
                out_specs=[vmem] * 3,
                scratch_shapes=[mixed_buf, rows_buf, buf, buf, pltpu.SemaphoreType.DMA((2,))],
                compiler_params=params,
                name="mix_gate",
            )(conv, far, channel_gain, channel_shift, out_weight, state, norm_gain, *remote(value_weight, gate_weight))
    return pl.pallas_call(
        functools.partial(mix_kernel, layer=layers - 1),
        in_specs=[vmem] * 6,
        out_shape=jax.ShapeDtypeStruct((tokens, width_in), bf16),
        out_specs=hbm,
        scratch_shapes=[mixed_buf, rows_buf, pltpu.SemaphoreType.DMA((columns,))],
        compiler_params=params,
        name="mix",
    )(conv, far, channel_gain, channel_shift, out_weight, state)


def solution(mesh):
    return jax.shard_map(
        per_device,
        mesh=mesh,
        in_specs=(
            P("sp", None),
            P(),
            P(None, None, "tp"),
            P(None, None, "tp"),
            P(None, None, "tp"),
            P(None, "tp"),
            P(),
            P(),
            P(),
        ),
        out_specs=P("sp", None),
        check_vma=False,
    )
```

time: 52.2 us -> 42.7 us (0.82)
  local copies, waits for them, and re-layouts: 7.11 us -> 0.1 us
  Pallas kernels: 23.9 us -> 18 us
  waiting for transfers between devices: 9.89 us -> 13.8 us
  starting transfers between devices: 10.7 us -> 10.1 us
    unnamed x50 -> x36, local copies, waits for them, and re-layouts: 7.1 us -> 0.1 us
    ppermute x4, waiting for transfers between devices: 7.66 us -> 11.6 us  [passed_along(): return lax.ppermute(value, axis, pairs)]
    pallas_call x2, Pallas kernels: 8.41 us -> 5.75 us  [the longest x1 3.5 us: per_device(): pl.pallas_call(first_gate_kernel, in_specs=[hbm] * 4, out_shape=gated_out...]
    pallas_call x1, Pallas kernels: 5.55 us -> 3.17 us  [per_device(): pl.pallas_call(functools.partial(mix_gate_kernel, layer=layer), in_specs=...]
    pallas_call x2, Pallas kernels: 6.38 us -> 5.53 us  [per_device(): pl.pallas_call(functools.partial(finish_kernel, layer=layer, pieces=len(p...]
  transfers between devices with their start and end apart: 6 -> 6, of which waited for: 5 -> 5; matrix products, arithmetic and copies ran while one was open for 0% -> 0% of each run, Pallas kernels for 7% -> 8%
where the time goes in v3:
time: 42.7 us; the launch traced here: 42.5 us
  Pallas kernels  18 us (42%)
  waiting for transfers between devices  13.8 us (32%)
  starting transfers between devices  10.1 us (24%)
  between operations  0.46 us (1%)
    ppermute x4, waiting for transfers between devices, passed_along(): return lax.ppermute(value, axis, pairs)  11.6 us
    ppermute x4, starting transfers between devices, passed_along(): return lax.ppermute(value, axis, pairs)  6.56 us
    pallas_call x2, Pallas kernels, per_device(): pl.pallas_call(functools.partial(finish_kernel, layer=layer, pieces=len(p...  5.53 us
    ppermute x2, starting transfers between devices, per_device(): far = lax.ppermute(conv, 'tp', [(0, 1), (1, 0)])  3.53 us
    pallas_call x1, Pallas kernels, per_device(): pl.pallas_call(first_gate_kernel, in_specs=[hbm] * 4, out_shape=gated_out...  3.5 us
    pallas_call x1, Pallas kernels, per_device(): pl.pallas_call(functools.partial(mix_gate_kernel, layer=layer), in_specs=...  3.17 us
    pallas_call x1, Pallas kernels, per_device(): pl.pallas_call(functools.partial(mix_kernel, layer=layers - 1), in_specs=...  2.25 us
    ppermute x2, waiting for transfers between devices, per_device(): far = lax.ppermute(conv, 'tp', [(0, 1), (1, 0)])  2.23 us
  transfers between devices with their start and end apart: 6, of which 5 were waited for; matrix products, arithmetic and copies ran while one was open for 0% of the time, Pallas kernels for 8%

profile of v3, /device:TPU:25, one launch (start us, length us, event | category | flops | bytes accessed | tf_op | source)
XLA Modules:
  0.0 42.5 jit_solution(5885293955034004870)
XLA Ops:
  0.0 0.0 copy-start.7
  0.0 0.0 copy-start.8
  0.0 0.0 copy-start.9
  0.0 0.0 copy-start.10
  0.0 0.0 copy-start.11
  0.0 0.0 copy-start.12
  0.0 0.0 copy-start.13
  0.1 0.0 copy-start.14
  0.1 0.0 copy-start.15
  0.1 0.0 copy-start.16
  0.1 0.0 copy-start.17
  0.1 0.0 copy-start.6
  0.1 3.5 %first_gate.1 = (bf16[64,256]{1,0:T(8,128)(2,1)S(1)}, bf16[448,256]{1,0:T(8,128)(2,1)S(1)}) custom-call(bf16[448,2048]{1,0:T(8,128)(2,1)} %state.1, f32[2,2048]{1,0:T(2,128)} %gain.1, bf16[2,2048,256]{2,1,0:T(8,128)(2,1)} %w_value.3, bf16[2,2048,256]{2,1,0:T(8,128)(2,1)} %w_gate.3), custom_call_target="tpu_custom_call" | custom-call | tf_op jit(solution)/shard_map/first_gate/pallas_call | solution.py:260
  3.6 1.3 %collective-permute-start = (bf16[64,256]{1,0:T(8,128)(2,1)S(1)}, bf16[64,256]{1,0:T(8,128)(2,1)S(1)}, u32[]{:S(2)}, u32[]{:S(2)}) collective-permute-start(bf16[64,256]{1,0:T(8,128)(2,1)S(1)} %get-tuple-element.19), channel_id=1, source_target_pairs={{0,4},{2,6},{4,8},{6,10},{8,12},{10,14},{12,16},{14,18},{16,20},{1... | collective-permute-start | bytes 98312 | tf_op jit(solution)/shard_map/ppermute | solution.py:18
  4.9 3.1 %collective-permute-start.1 = (bf16[448,256]{1,0:T(8,128)(2,1)S(1)}, bf16[448,256]{1,0:T(8,128)(2,1)S(1)}, u32[]{:S(2)}, u32[]{:S(2)}) collective-permute-start(bf16[448,256]{1,0:T(8,128)(2,1)S(1)} %get-tuple-element.17.gated), channel_id=1, source_target_pairs={{0,2},{2,4},{4,6},{6,8},{8,10},{10,12},{12,14},{14,16},{16,18},{18... | collective-permute-start | bytes 688136 | tf_op jit(solution)/shard_map/ppermute | solution.py:18
  8.0 0.0 copy-done.7
  8.0 0.0 copy-done.8
  8.1 0.0 copy-done.9
  8.1 0.0 copy-done.10
  8.1 0.0 copy-done.11
  8.1 0.0 copy-done.12
  8.1 0.0 copy-done.13
  8.1 0.0 copy-done.14
  8.1 0.0 copy-done.15
  8.1 0.0 copy-done.16
  8.1 0.0 copy-done.17
  8.1 0.0 copy-done.6
  8.2 2.1 %prep.1 = (bf16[1024,1024]{1,0:T(8,128)(2,1)S(1)}, bf16[1024,1024]{1,0:T(8,128)(2,1)S(1)}, bf16[448,2048]{1,0:T(8,128)(2,1)S(1)}, f32[2,1024,256]{2,1,0:T(8,128)S(1)}) custom-call(f32[16,512]{1,0:T(8,128)S(1)} %copy-done.17, f32[16,512]{1,0:T(8,128)S(1)} %copy-done.16, f32[32,512]{1,0:T(8,128)S(1)} %copy-done.12, f32[32,512]{1,0:T(8,128)S(1)} %copy-done.11, ...), custom_call_target="tpu_custom_call" | custom-call | flops 2147483648 | bytes 8388608 | tf_op jit(solution)/shard_map/prep/pallas_call | solution.py:244
  10.3 0.0 copy-start.5
  10.3 0.7 %own_part.2.refs_2_ = f32[1024,256]{1,0:T(8,128)S(1)} custom-call(bf16[1024,1024]{1,0:T(8,128)(2,1)S(1)} %get-tuple-element.16.matrix, bf16[448,256]{1,0:T(8,128)(2,1)S(1)} %get-tuple-element.17.gated), custom_call_target="tpu_custom_call" | custom-call | flops 939524096 | bytes 4194304 | tf_op jit(solution)/shard_map/own_part/pallas_call | solution.py:281
  11.0 0.0 collective-permute-done.refs_5_
  11.0 3.8 %collective-permute-done.1.refs_6_ = bf16[448,256]{1,0:T(8,128)(2,1)S(1)} collective-permute-done((bf16[448,256]{1,0:T(8,128)(2,1)S(1)}, bf16[448,256]{1,0:T(8,128)(2,1)S(1)}, u32[]{:S(2)}, u32[]{:S(2)}) %collective-permute-start.1) | collective-permute-done | bytes 229408 | tf_op jit(solution)/shard_map/ppermute | solution.py:18
  14.8 0.0 copy-done.5
  14.8 0.0 copy-start
  14.8 0.0 copy-start.1
  14.8 0.0 copy-start.2
  14.8 0.0 copy-start.3
  14.8 0.0 copy-start.4
  14.8 2.8 %finish.2.own = bf16[448,256]{1,0:T(8,128)(2,1)S(1)} custom-call(bf16[1024,1024]{1,0:T(8,128)(2,1)S(1)} %get-tuple-element.14.refs_0_, f32[2,1024,256]{2,1,0:T(8,128)S(1)} %get-tuple-element.15.refs_1_, f32[1024,256]{1,0:T(8,128)S(1)} %own_part.2.refs_2_, bf16[448,2048]{1,0:T(8,128)(2,1)S(1)} %get-tuple-element.18.refs_3_, f32[2,256]{1,0:T(2,128)S(1)} %copy-done.5, ...), custom_call_target="tpu_custom_call" | custom-call | flops 1073741824 | bytes 4194304 | tf_op jit(solution)/shard_map/finish/pallas_call | solution.py:289
  17.6 1.9 %collective-permute-start.2 = (bf16[448,256]{1,0:T(8,128)(2,1)S(1)}, bf16[448,256]{1,0:T(8,128)(2,1)S(1)}, u32[]{:S(2)}, u32[]{:S(2)}) collective-permute-start(bf16[448,256]{1,0:T(8,128)(2,1)S(1)} %finish.2.own), channel_id=1, source_target_pairs={{0,1},{1,0},{2,3},{3,2},{4,5},{5,4},{6,7},{7,6},{8,9},{9,8},{10,11... | collective-permute-start | bytes 688136 | tf_op jit(solution)/shard_map/ppermute | solution.py:298
  19.5 1.1 %collective-permute-done.2.far = bf16[448,256]{1,0:T(8,128)(2,1)S(1)} collective-permute-done((bf16[448,256]{1,0:T(8,128)(2,1)S(1)}, bf16[448,256]{1,0:T(8,128)(2,1)S(1)}, u32[]{:S(2)}, u32[]{:S(2)}) %collective-permute-start.2) | collective-permute-done | bytes 229408 | tf_op jit(solution)/shard_map/ppermute | solution.py:298
  20.6 0.0 copy-done
  20.6 0.0 copy-done.1
  20.6 0.0 copy-done.2
  20.6 0.0 copy-done.3
  20.6 0.0 copy-done.4
  20.6 3.2 %mix_gate.1 = (bf16[448,2048]{1,0:T(8,128)(2,1)S(1)}, bf16[448,256]{1,0:T(8,128)(2,1)S(1)}, bf16[64,256]{1,0:T(8,128)(2,1)S(1)}) custom-call(bf16[448,256]{1,0:T(8,128)(2,1)S(1)} %finish.2.own, bf16[448,256]{1,0:T(8,128)(2,1)S(1)} %collective-permute-done.2.far, f32[2,512]{1,0:T(2,128)S(1)} %copy-done.3, f32[2,512]{1,0:T(2,128)S(1)} %copy-done.4, ...), custom_call_target="tpu_custom_call" | custom-call | tf_op jit(solution)/shard_map/mix_gate/pallas_call | solution.py:300
  23.8 1.9 %collective-permute-start.4 = (bf16[448,256]{1,0:T(8,128)(2,1)S(1)}, bf16[448,256]{1,0:T(8,128)(2,1)S(1)}, u32[]{:S(2)}, u32[]{:S(2)}) collective-permute-start(bf16[448,256]{1,0:T(8,128)(2,1)S(1)} %get-tuple-element.20.gated), channel_id=1, source_target_pairs={{0,2},{2,4},{4,6},{6,8},{8,10},{10,12},{12,14},{14,16},{16,18},{18... | collective-permute-start | bytes 688136 | tf_op jit(solution)/shard_map/ppermute | solution.py:18
  25.7 0.2 collective-permute-start.3
  26.0 0.7 %own_part.3.refs_2_ = f32[1024,256]{1,0:T(8,128)S(1)} custom-call(bf16[1024,1024]{1,0:T(8,128)(2,1)S(1)} %get-tuple-element.16.matrix, bf16[448,256]{1,0:T(8,128)(2,1)S(1)} %get-tuple-element.20.gated), custom_call_target="tpu_custom_call" | custom-call | flops 939524096 | bytes 4194304 | tf_op jit(solution)/shard_map/own_part/pallas_call | solution.py:281
  26.7 5.0 %collective-permute-done.3.refs_5_ = bf16[64,256]{1,0:T(8,128)(2,1)S(1)} collective-permute-done((bf16[64,256]{1,0:T(8,128)(2,1)S(1)}, bf16[64,256]{1,0:T(8,128)(2,1)S(1)}, u32[]{:S(2)}, u32[]{:S(2)}) %collective-permute-start.3) | collective-permute-done | bytes 32800 | tf_op jit(solution)/shard_map/ppermute | solution.py:18
  31.7 2.9 %collective-permute-done.4.refs_6_ = bf16[448,256]{1,0:T(8,128)(2,1)S(1)} collective-permute-done((bf16[448,256]{1,0:T(8,128)(2,1)S(1)}, bf16[448,256]{1,0:T(8,128)(2,1)S(1)}, u32[]{:S(2)}, u32[]{:S(2)}) %collective-permute-start.4) | collective-permute-done | bytes 229408 | tf_op jit(solution)/shard_map/ppermute | solution.py:18
  34.5 2.8 %finish.3.own = bf16[448,256]{1,0:T(8,128)(2,1)S(1)} custom-call(bf16[1024,1024]{1,0:T(8,128)(2,1)S(1)} %get-tuple-element.14.refs_0_, f32[2,1024,256]{2,1,0:T(8,128)S(1)} %get-tuple-element.15.refs_1_, f32[1024,256]{1,0:T(8,128)S(1)} %own_part.3.refs_2_, bf16[448,2048]{1,0:T(8,128)(2,1)S(1)} %get-tuple-element.18.refs_3_, f32[2,256]{1,0:T(2,128)S(1)} %copy-done.5, ...), custom_call_target="tpu_custom_call" | custom-call | flops 1073741824 | bytes 4194304 | tf_op jit(solution)/shard_map/finish/pallas_call | solution.py:289
  37.3 1.6 %collective-permute-start.5 = (bf16[448,256]{1,0:T(8,128)(2,1)S(1)}, bf16[448,256]{1,0:T(8,128)(2,1)S(1)}, u32[]{:S(2)}, u32[]{:S(2)}) collective-permute-start(bf16[448,256]{1,0:T(8,128)(2,1)S(1)} %finish.3.own), channel_id=1, source_target_pairs={{0,1},{1,0},{2,3},{3,2},{4,5},{5,4},{6,7},{7,6},{8,9},{9,8},{10,11... | collective-permute-start | bytes 688136 | tf_op jit(solution)/shard_map/ppermute | solution.py:298
  38.9 1.1 %collective-permute-done.5.far = bf16[448,256]{1,0:T(8,128)(2,1)S(1)} collective-permute-done((bf16[448,256]{1,0:T(8,128)(2,1)S(1)}, bf16[448,256]{1,0:T(8,128)(2,1)S(1)}, u32[]{:S(2)}, u32[]{:S(2)}) %collective-permute-start.5) | collective-permute-done | bytes 229408 | tf_op jit(solution)/shard_map/ppermute | solution.py:298
  40.1 2.3 %mix.1 = bf16[448,2048]{1,0:T(8,128)(2,1)} custom-call(bf16[448,256]{1,0:T(8,128)(2,1)S(1)} %finish.3.own, bf16[448,256]{1,0:T(8,128)(2,1)S(1)} %collective-permute-done.5.far, f32[2,512]{1,0:T(2,128)S(1)} %copy-done.3, f32[2,512]{1,0:T(2,128)S(1)} %copy-done.4, bf16[2,512,2048]{2,1,0:T(8,128)(2,1)S(1)} %copy-done, bf16[448,2048]{1,0:T(8,128)(2,1)S(1)} %get-tuple-element.22.state), custom_call_target="tpu_custom_call" | custom-call | tf_op jit(solution)/shard_map/mix/pallas_call | solution.py:309
Async XLA Ops:
  0.0 8.0 %copy-start.7 = (f32[32,512]{1,0:T(8,128)S(1)}, f32[32,512]{1,0:T(8,128)}, u32[]{:S(2)}) copy-start(f32[32,512]{1,0:T(8,128)} %constant.32.clone.refs_11_) | copy-start | bytes 196612
  0.0 8.0 %copy-start.8 = (f32[32,512]{1,0:T(8,128)S(1)}, f32[32,512]{1,0:T(8,128)}, u32[]{:S(2)}) copy-start(f32[32,512]{1,0:T(8,128)} %constant.31.clone.refs_10_) | copy-start | bytes 196612
  0.0 8.1 %copy-start.9 = (f32[32,512]{1,0:T(8,128)S(1)}, f32[32,512]{1,0:T(8,128)}, u32[]{:S(2)}) copy-start(f32[32,512]{1,0:T(8,128)} %constant.28.clone.refs_7_) | copy-start | bytes 196612
  0.0 8.1 %copy-start.10 = (f32[32,512]{1,0:T(8,128)S(1)}, f32[32,512]{1,0:T(8,128)}, u32[]{:S(2)}) copy-start(f32[32,512]{1,0:T(8,128)} %constant.27.clone.refs_6_) | copy-start | bytes 196612
  0.0 8.1 %copy-start.11 = (f32[32,512]{1,0:T(8,128)S(1)}, f32[32,512]{1,0:T(8,128)}, u32[]{:S(2)}) copy-start(f32[32,512]{1,0:T(8,128)} %constant.25.clone.refs_3_) | copy-start | bytes 196612
  0.0 8.1 %copy-start.12 = (f32[32,512]{1,0:T(8,128)S(1)}, f32[32,512]{1,0:T(8,128)}, u32[]{:S(2)}) copy-start(f32[32,512]{1,0:T(8,128)} %constant.24.clone.refs_2_) | copy-start | bytes 196612
  0.0 8.1 %copy-start.13 = (f32[14,512]{1,0:T(8,128)S(1)}, f32[14,512]{1,0:T(8,128)}, u32[]{:S(2)}) copy-start(f32[14,512]{1,0:T(8,128)} %constant.30.clone.refs_9_) | copy-start | bytes 86020
  0.1 8.1 %copy-start.14 = (f32[14,512]{1,0:T(8,128)S(1)}, f32[14,512]{1,0:T(8,128)}, u32[]{:S(2)}) copy-start(f32[14,512]{1,0:T(8,128)} %constant.29.clone.refs_8_) | copy-start | bytes 86020
  0.1 8.0 %copy-start.15 = (f32[16,512]{1,0:T(8,128)S(1)}, f32[16,512]{1,0:T(8,128)}, u32[]{:S(2)}) copy-start(f32[16,512]{1,0:T(8,128)} %constant.26.clone.refs_5_) | copy-start | bytes 98308
  0.1 8.0 %copy-start.16 = (f32[16,512]{1,0:T(8,128)S(1)}, f32[16,512]{1,0:T(8,128)}, u32[]{:S(2)}) copy-start(f32[16,512]{1,0:T(8,128)} %constant.23.clone.refs_1_.refs_4_) | copy-start | bytes 98308
  0.1 8.0 %copy-start.17 = (f32[16,512]{1,0:T(8,128)S(1)}, f32[16,512]{1,0:T(8,128)}, u32[]{:S(2)}) copy-start(f32[16,512]{1,0:T(8,128)} %constant.22.clone.refs_0_) | copy-start | bytes 98308
  0.1 8.0 %copy-start.6 = (bf16[2,512,256]{2,1,0:T(8,128)(2,1)S(1)}, bf16[2,512,256]{2,1,0:T(8,128)(2,1)}, u32[]{:S(2)}) copy-start(bf16[2,512,256]{2,1,0:T(8,128)(2,1)} %refs_12_.1) | copy-start | bytes 1572868
  3.6 7.4 %collective-permute-start = (bf16[64,256]{1,0:T(8,128)(2,1)S(1)}, bf16[64,256]{1,0:T(8,128)(2,1)S(1)}, u32[]{:S(2)}, u32[]{:S(2)}) collective-permute-start(bf16[64,256]{1,0:T(8,128)(2,1)S(1)} %get-tuple-element.19), channel_id=1, source_target_pairs={{0,4},{2,6},{4,8},{6,10},{8,12},{10,14},{12,16},{14,18},{16,20},{1... | collective-permute-start | bytes 98312 | tf_op jit(solution)/shard_map/ppermute | solution.py:18
  4.9 9.9 %collective-permute-start.1 = (bf16[448,256]{1,0:T(8,128)(2,1)S(1)}, bf16[448,256]{1,0:T(8,128)(2,1)S(1)}, u32[]{:S(2)}, u32[]{:S(2)}) collective-permute-start(bf16[448,256]{1,0:T(8,128)(2,1)S(1)} %get-tuple-element.17.gated), channel_id=1, source_target_pairs={{0,2},{2,4},{4,6},{6,8},{8,10},{10,12},{12,14},{14,16},{16,18},{18... | collective-permute-start | bytes 688136 | tf_op jit(solution)/shard_map/ppermute | solution.py:18
  10.3 4.5 %copy-start.5 = (f32[2,256]{1,0:T(2,128)S(1)}, f32[2,256]{1,0:T(2,128)}, u32[]{:S(2)}) copy-start(f32[2,256]{1,0:T(2,128)} %refs_4_.4) | copy-start | bytes 6148
  14.8 5.8 %copy-start = (bf16[2,512,2048]{2,1,0:T(8,128)(2,1)S(1)}, bf16[2,512,2048]{2,1,0:T(8,128)(2,1)}, u32[]{:S(2)}) copy-start(bf16[2,512,2048]{2,1,0:T(8,128)(2,1)} %w_out.3) | copy-start | bytes 12582916
  14.8 5.8 %copy-start.1 = (bf16[448,2048]{1,0:T(8,128)(2,1)S(1)}, bf16[448,2048]{1,0:T(8,128)(2,1)}, u32[]{:S(2)}) copy-start(bf16[448,2048]{1,0:T(8,128)(2,1)} %state.1) | copy-start | bytes 5505028
  14.8 5.8 %copy-start.2 = (f32[2,2048]{1,0:T(2,128)S(1)}, f32[2,2048]{1,0:T(2,128)}, u32[]{:S(2)}) copy-start(f32[2,2048]{1,0:T(2,128)} %gain.1) | copy-start | bytes 49156
  14.8 5.8 %copy-start.3 = (f32[2,512]{1,0:T(2,128)S(1)}, f32[2,512]{1,0:T(2,128)}, u32[]{:S(2)}) copy-start(f32[2,512]{1,0:T(2,128)} %ch_gain.3) | copy-start | bytes 12292
  14.8 5.8 %copy-start.4 = (f32[2,512]{1,0:T(2,128)S(1)}, f32[2,512]{1,0:T(2,128)}, u32[]{:S(2)}) copy-start(f32[2,512]{1,0:T(2,128)} %ch_shift.3) | copy-start | bytes 12292
  17.6 3.0 %collective-permute-start.2 = (bf16[448,256]{1,0:T(8,128)(2,1)S(1)}, bf16[448,256]{1,0:T(8,128)(2,1)S(1)}, u32[]{:S(2)}, u32[]{:S(2)}) collective-permute-start(bf16[448,256]{1,0:T(8,128)(2,1)S(1)} %finish.2.own), channel_id=1, source_target_pairs={{0,1},{1,0},{2,3},{3,2},{4,5},{5,4},{6,7},{7,6},{8,9},{9,8},{10,11... | collective-permute-start | bytes 688136 | tf_op jit(solution)/shard_map/ppermute | solution.py:298
  23.8 10.7 %collective-permute-start.4 = (bf16[448,256]{1,0:T(8,128)(2,1)S(1)}, bf16[448,256]{1,0:T(8,128)(2,1)S(1)}, u32[]{:S(2)}, u32[]{:S(2)}) collective-permute-start(bf16[448,256]{1,0:T(8,128)(2,1)S(1)} %get-tuple-element.20.gated), channel_id=1, source_target_pairs={{0,2},{2,4},{4,6},{6,8},{8,10},{10,12},{12,14},{14,16},{16,18},{18... | collective-permute-start | bytes 688136 | tf_op jit(solution)/shard_map/ppermute | solution.py:18
  25.7 5.9 %collective-permute-start.3 = (bf16[64,256]{1,0:T(8,128)(2,1)S(1)}, bf16[64,256]{1,0:T(8,128)(2,1)S(1)}, u32[]{:S(2)}, u32[]{:S(2)}) collective-permute-start(bf16[64,256]{1,0:T(8,128)(2,1)S(1)} %get-tuple-element.21), channel_id=1, source_target_pairs={{0,4},{2,6},{4,8},{6,10},{8,12},{10,14},{12,16},{14,18},{16,20},{1... | collective-permute-start | bytes 98312 | tf_op jit(solution)/shard_map/ppermute | solution.py:18
  37.3 2.8 %collective-permute-start.5 = (bf16[448,256]{1,0:T(8,128)(2,1)S(1)}, bf16[448,256]{1,0:T(8,128)(2,1)S(1)}, u32[]{:S(2)}, u32[]{:S(2)}) collective-permute-start(bf16[448,256]{1,0:T(8,128)(2,1)S(1)} %finish.3.own), channel_id=1, source_target_pairs={{0,1},{1,0},{2,3},{3,2},{4,5},{5,4},{6,7},{7,6},{8,9},{9,8},{10,11... | collective-permute-start | bytes 688136 | tf_op jit(solution)/shard_map/ppermute | solution.py:298

commit v4 on v3

--- a/solution.py
+++ b/solution.py
@@ -28,10 +28,11 @@
     gates = dot(normed[...], w_gate[...])
     out = (values * jax.nn.sigmoid(gates)).astype(jnp.bfloat16)
     gated[...] = out
-    tail[...] = out[out.shape[0] - tail.shape[0] :]
-
-
-def first_gate_kernel(stream, gain_h, w_value, w_gate, tail, gated, state, normed, gain, v_buf, g_buf, sems):
+    if tail is not None:
+        tail[...] = out[out.shape[0] - tail.shape[0] :]
+
+
+def first_gate_kernel(stream, gain_h, w_value, w_gate, gated, state, normed, gain, v_buf, g_buf, sems):
     total = state.shape[0]
     pieces = chunks(total, 64)
     copies = [pltpu.make_async_copy(gain_h, gain, sems.at[0])]
@@ -51,7 +52,7 @@
             normed[rows, :] = (values * scale * gain[0:1, :]).astype(jnp.bfloat16)
     copies[-2].wait()
     copies[-1].wait()
-    gate_all(normed, v_buf, g_buf, gated, tail)
+    gate_all(normed, v_buf, g_buf, gated, None)
 
 
 def mix_all(first, other, gain, shift, mixed):
@@ -153,7 +154,8 @@
 
 def prep_kernel(*refs):
     own_t, halo_t, back_t = refs[0:4], refs[4:8], refs[8:12]
-    taps, own, halo, back, spectra = refs[12:17]
+    taps, gated, own, halo, back, spectra, tail = refs[12:19]
+    tail[...] = gated[gated.shape[0] - tail.shape[0] :, :]
     forward_matrix(halo_t, halo)
     for layer in range(taps.shape[0]):
         t = taps[layer]
@@ -241,27 +243,14 @@
     def remote(*arrays):
         return [pltpu.with_memory_space_constraint(a, pltpu.HBM) for a in arrays]
 
-    own_m, halo_m, back_m, spectra = pl.pallas_call(
-        prep_kernel,
-        out_shape=[
-            jax.ShapeDtypeStruct((size, 2 * span), bf16),
-            jax.ShapeDtypeStruct((size, 2 * halo_rows), bf16),
-            jax.ShapeDtypeStruct((tokens, 2 * size), bf16),
-            jax.ShapeDtypeStruct((layers, size, chans), f32),
-        ],
-        cost_estimate=cost(8 * layers * size * halo_rows * chans, 8 << 20),
-        compiler_params=pltpu.CompilerParams(vmem_limit_bytes=LIMIT),
-        name="prep",
-    )(*own_tab, *halo_tab, *back_tab, taps)
-
     rows_buf = pltpu.VMEM((tokens, width_in), bf16)
     mixed_buf = pltpu.VMEM((tokens, out_weight.shape[1]), bf16)
     gated_out = [pltpu.VMEM((tokens, chans), bf16), pltpu.VMEM((last, chans), bf16)]
-    tail, own_gated = pl.pallas_call(
+    own_gated = pl.pallas_call(
         first_gate_kernel,
         in_specs=[hbm] * 4,
-        out_shape=gated_out[::-1],
-        out_specs=[vmem] * 2,
+        out_shape=gated_out[0],
+        out_specs=vmem,
         scratch_shapes=[
             rows_buf,
             rows_buf,
@@ -273,6 +262,20 @@
         compiler_params=params,
         name="first_gate",
     )(*remote(stream, norm_gain, value_weight, gate_weight))
+    own_m, halo_m, back_m, spectra, tail = pl.pallas_call(
+        prep_kernel,
+        out_shape=[
+            jax.ShapeDtypeStruct((size, 2 * span), bf16),
+            jax.ShapeDtypeStruct((size, 2 * halo_rows), bf16),
+            jax.ShapeDtypeStruct((tokens, 2 * size), bf16),
+            jax.ShapeDtypeStruct((layers, size, chans), f32),
+            pltpu.VMEM((last, chans), bf16),
+        ],
+        cost_estimate=cost(8 * layers * size * halo_rows * chans, 8 << 20),
+        compiler_params=pltpu.CompilerParams(vmem_limit_bytes=LIMIT),
+        name="prep",
+    )(*own_tab, *halo_tab, *back_tab, taps, own_gated)
+
     state = stream
     for layer in range(layers):
         pieces = []

time: 42.7 us -> 42.2 us (0.988)
  waiting for transfers between devices: 13.8 us -> 12.5 us
  starting transfers between devices: 10.1 us -> 10.8 us
    ppermute x4, waiting for transfers between devices: 11.6 us -> 10.3 us  [passed_along(): return lax.ppermute(value, axis, pairs)]
  transfers between devices with their start and end apart: 6 -> 6, of which waited for: 5 -> 6; matrix products, arithmetic and copies ran while one was open for 0% -> 0% of each run, Pallas kernels for 8% -> 9%
where the time goes in v4:
time: 42.2 us; the launch traced here: 41.9 us
  Pallas kernels  18 us (43%)
  waiting for transfers between devices  12.5 us (30%)
  starting transfers between devices  10.8 us (26%)
  between operations  0.44 us (1%)
    ppermute x4, waiting for transfers between devices, passed_along(): return lax.ppermute(value, axis, pairs)  10.3 us
    ppermute x4, starting transfers between devices, passed_along(): return lax.ppermute(value, axis, pairs)  6.94 us
    pallas_call x2, Pallas kernels, per_device(): pl.pallas_call(functools.partial(finish_kernel, layer=layer, pieces=len(p...  5.53 us
    ppermute x2, starting transfers between devices, per_device(): far = lax.ppermute(conv, 'tp', [(0, 1), (1, 0)])  3.91 us
    pallas_call x1, Pallas kernels, per_device(): pl.pallas_call(first_gate_kernel, in_specs=[hbm] * 4, out_shape=gated_out...  3.5 us
    pallas_call x1, Pallas kernels, per_device(): pl.pallas_call(functools.partial(mix_gate_kernel, layer=layer), in_specs=...  3.16 us
    pallas_call x1, Pallas kernels, per_device(): pl.pallas_call(functools.partial(mix_kernel, layer=layers - 1), in_specs=...  2.25 us
    ppermute x2, waiting for transfers between devices, per_device(): far = lax.ppermute(conv, 'tp', [(0, 1), (1, 0)])  2.23 us
  transfers between devices with their start and end apart: 6, of which 6 were waited for; matrix products, arithmetic and copies ran while one was open for 0% of the time, Pallas kernels for 9%

profile of v4, /device:TPU:25, one launch (start us, length us, event | category | flops | bytes accessed | tf_op | source)
XLA Modules:
  0.0 41.9 jit_solution(553675152872789756)
XLA Ops:
  0.0 0.0 copy-start.7
  0.0 0.0 copy-start.8
  0.0 0.0 copy-start.9
  0.0 0.0 copy-start.10
  0.0 0.0 copy-start.11
  0.0 0.0 copy-start.12
  0.0 0.0 copy-start.13
  0.1 0.0 copy-start.14
  0.1 0.0 copy-start.15
  0.1 0.0 copy-start.16
  0.1 0.0 copy-start.17
  0.1 0.0 copy-start.6
  0.1 3.5 %first_gate.1.refs_13_.gated = bf16[448,256]{1,0:T(8,128)(2,1)S(1)} custom-call(bf16[448,2048]{1,0:T(8,128)(2,1)} %state.1, f32[2,2048]{1,0:T(2,128)} %gain.1, bf16[2,2048,256]{2,1,0:T(8,128)(2,1)} %w_value.3, bf16[2,2048,256]{2,1,0:T(8,128)(2,1)} %w_gate.3), custom_call_target="tpu_custom_call" | custom-call | tf_op jit(solution)/shard_map/first_gate/pallas_call | solution.py:249
  3.6 3.1 %collective-permute-start.1 = (bf16[448,256]{1,0:T(8,128)(2,1)S(1)}, bf16[448,256]{1,0:T(8,128)(2,1)S(1)}, u32[]{:S(2)}, u32[]{:S(2)}) collective-permute-start(bf16[448,256]{1,0:T(8,128)(2,1)S(1)} %first_gate.1.refs_13_.gated), channel_id=1, source_target_pairs={{0,2},{2,4},{4,6},{6,8},{8,10},{10,12},{12,14},{14,16},{16,18},{18... | collective-permute-start | bytes 688136 | tf_op jit(solution)/shard_map/ppermute | solution.py:18
  6.8 0.0 copy-done.7
  6.8 0.0 copy-done.8
  6.8 0.0 copy-done.9
  6.8 0.0 copy-done.10
  6.8 0.0 copy-done.11
  6.8 0.0 copy-done.12
  6.8 0.0 copy-done.13
  6.8 0.0 copy-done.14
  6.8 0.0 copy-done.15
  6.8 0.0 copy-done.16
  6.9 0.0 copy-done.17
  6.9 0.0 copy-done.6
  6.9 2.1 %prep.1 = (bf16[1024,1024]{1,0:T(8,128)(2,1)S(1)}, bf16[1024,1024]{1,0:T(8,128)(2,1)S(1)}, bf16[448,2048]{1,0:T(8,128)(2,1)S(1)}, f32[2,1024,256]{2,1,0:T(8,128)S(1)}, bf16[64,256]{1,0:T(8,128)(2,1)S(1)}) custom-call(f32[16,512]{1,0:T(8,128)S(1)} %copy-done.17, f32[16,512]{1,0:T(8,128)S(1)} %copy-done.16, f32[32,512]{1,0:T(8,128)S(1)} %copy-done.12, ...), custom_call_target="tpu_custom_call" | custom-call | flops 2147483648 | bytes 8388608 | tf_op jit(solution)/shard_map/prep/pallas_call | solution.py:265
  9.0 0.0 copy-start.5
  9.0 1.3 %collective-permute-start = (bf16[64,256]{1,0:T(8,128)(2,1)S(1)}, bf16[64,256]{1,0:T(8,128)(2,1)S(1)}, u32[]{:S(2)}, u32[]{:S(2)}) collective-permute-start(bf16[64,256]{1,0:T(8,128)(2,1)S(1)} %get-tuple-element.17), channel_id=1, source_target_pairs={{0,4},{2,6},{4,8},{6,10},{8,12},{10,14},{12,16},{14,18},{16,20},{1... | collective-permute-start | bytes 98312 | tf_op jit(solution)/shard_map/ppermute | solution.py:18
  10.3 0.7 %own_part.2.refs_2_ = f32[1024,256]{1,0:T(8,128)S(1)} custom-call(bf16[1024,1024]{1,0:T(8,128)(2,1)S(1)} %get-tuple-element.15.matrix, bf16[448,256]{1,0:T(8,128)(2,1)S(1)} %first_gate.1.refs_13_.gated), custom_call_target="tpu_custom_call" | custom-call | flops 939524096 | bytes 4194304 | tf_op jit(solution)/shard_map/own_part/pallas_call | solution.py:284
  11.0 2.5 %collective-permute-done.refs_5_ = bf16[64,256]{1,0:T(8,128)(2,1)S(1)} collective-permute-done((bf16[64,256]{1,0:T(8,128)(2,1)S(1)}, bf16[64,256]{1,0:T(8,128)(2,1)S(1)}, u32[]{:S(2)}, u32[]{:S(2)}) %collective-permute-start) | collective-permute-done | bytes 32800 | tf_op jit(solution)/shard_map/ppermute | solution.py:18
  13.5 0.3 collective-permute-done.1.refs_6_
  13.9 0.0 copy-done.5
  13.9 0.0 copy-start
  13.9 0.0 copy-start.1
  13.9 0.0 copy-start.2
  13.9 0.0 copy-start.3
  13.9 0.0 copy-start.4
  13.9 2.8 %finish.2.own = bf16[448,256]{1,0:T(8,128)(2,1)S(1)} custom-call(bf16[1024,1024]{1,0:T(8,128)(2,1)S(1)} %get-tuple-element.13.refs_0_, f32[2,1024,256]{2,1,0:T(8,128)S(1)} %get-tuple-element.14.refs_1_, f32[1024,256]{1,0:T(8,128)S(1)} %own_part.2.refs_2_, bf16[448,2048]{1,0:T(8,128)(2,1)S(1)} %get-tuple-element.16.refs_3_, f32[2,256]{1,0:T(2,128)S(1)} %copy-done.5, ...), custom_call_target="tpu_custom_call" | custom-call | flops 1073741824 | bytes 4194304 | tf_op jit(solution)/shard_map/finish/pallas_call | solution.py:292
  16.7 2.2 %collective-permute-start.2 = (bf16[448,256]{1,0:T(8,128)(2,1)S(1)}, bf16[448,256]{1,0:T(8,128)(2,1)S(1)}, u32[]{:S(2)}, u32[]{:S(2)}) collective-permute-start(bf16[448,256]{1,0:T(8,128)(2,1)S(1)} %finish.2.own), channel_id=1, source_target_pairs={{0,1},{1,0},{2,3},{3,2},{4,5},{5,4},{6,7},{7,6},{8,9},{9,8},{10,11... | collective-permute-start | bytes 688136 | tf_op jit(solution)/shard_map/ppermute | solution.py:301
  18.9 1.1 %collective-permute-done.2.far = bf16[448,256]{1,0:T(8,128)(2,1)S(1)} collective-permute-done((bf16[448,256]{1,0:T(8,128)(2,1)S(1)}, bf16[448,256]{1,0:T(8,128)(2,1)S(1)}, u32[]{:S(2)}, u32[]{:S(2)}) %collective-permute-start.2) | collective-permute-done | bytes 229408 | tf_op jit(solution)/shard_map/ppermute | solution.py:301
  20.0 0.0 copy-done
  20.0 0.0 copy-done.1
  20.0 0.0 copy-done.2
  20.0 0.0 copy-done.3
  20.1 0.0 copy-done.4
  20.1 3.2 %mix_gate.1 = (bf16[448,2048]{1,0:T(8,128)(2,1)S(1)}, bf16[448,256]{1,0:T(8,128)(2,1)S(1)}, bf16[64,256]{1,0:T(8,128)(2,1)S(1)}) custom-call(bf16[448,256]{1,0:T(8,128)(2,1)S(1)} %finish.2.own, bf16[448,256]{1,0:T(8,128)(2,1)S(1)} %collective-permute-done.2.far, f32[2,512]{1,0:T(2,128)S(1)} %copy-done.3, f32[2,512]{1,0:T(2,128)S(1)} %copy-done.4, ...), custom_call_target="tpu_custom_call" | custom-call | tf_op jit(solution)/shard_map/mix_gate/pallas_call | solution.py:303
  23.2 2.2 %collective-permute-start.4 = (bf16[448,256]{1,0:T(8,128)(2,1)S(1)}, bf16[448,256]{1,0:T(8,128)(2,1)S(1)}, u32[]{:S(2)}, u32[]{:S(2)}) collective-permute-start(bf16[448,256]{1,0:T(8,128)(2,1)S(1)} %get-tuple-element.18.gated), channel_id=1, source_target_pairs={{0,2},{2,4},{4,6},{6,8},{8,10},{10,12},{12,14},{14,16},{16,18},{18... | collective-permute-start | bytes 688136 | tf_op jit(solution)/shard_map/ppermute | solution.py:18
  25.5 0.3 collective-permute-start.3
  25.8 0.7 %own_part.3.refs_2_ = f32[1024,256]{1,0:T(8,128)S(1)} custom-call(bf16[1024,1024]{1,0:T(8,128)(2,1)S(1)} %get-tuple-element.15.matrix, bf16[448,256]{1,0:T(8,128)(2,1)S(1)} %get-tuple-element.18.gated), custom_call_target="tpu_custom_call" | custom-call | flops 939524096 | bytes 4194304 | tf_op jit(solution)/shard_map/own_part/pallas_call | solution.py:284
  26.5 2.9 %collective-permute-done.3.refs_5_ = bf16[64,256]{1,0:T(8,128)(2,1)S(1)} collective-permute-done((bf16[64,256]{1,0:T(8,128)(2,1)S(1)}, bf16[64,256]{1,0:T(8,128)(2,1)S(1)}, u32[]{:S(2)}, u32[]{:S(2)}) %collective-permute-start.3) | collective-permute-done | bytes 32800 | tf_op jit(solution)/shard_map/ppermute | solution.py:18
  29.4 4.6 %collective-permute-done.4.refs_6_ = bf16[448,256]{1,0:T(8,128)(2,1)S(1)} collective-permute-done((bf16[448,256]{1,0:T(8,128)(2,1)S(1)}, bf16[448,256]{1,0:T(8,128)(2,1)S(1)}, u32[]{:S(2)}, u32[]{:S(2)}) %collective-permute-start.4) | collective-permute-done | bytes 229408 | tf_op jit(solution)/shard_map/ppermute | solution.py:18
  33.9 2.8 %finish.3.own = bf16[448,256]{1,0:T(8,128)(2,1)S(1)} custom-call(bf16[1024,1024]{1,0:T(8,128)(2,1)S(1)} %get-tuple-element.13.refs_0_, f32[2,1024,256]{2,1,0:T(8,128)S(1)} %get-tuple-element.14.refs_1_, f32[1024,256]{1,0:T(8,128)S(1)} %own_part.3.refs_2_, bf16[448,2048]{1,0:T(8,128)(2,1)S(1)} %get-tuple-element.16.refs_3_, f32[2,256]{1,0:T(2,128)S(1)} %copy-done.5, ...), custom_call_target="tpu_custom_call" | custom-call | flops 1073741824 | bytes 4194304 | tf_op jit(solution)/shard_map/finish/pallas_call | solution.py:292
  36.7 1.7 %collective-permute-start.5 = (bf16[448,256]{1,0:T(8,128)(2,1)S(1)}, bf16[448,256]{1,0:T(8,128)(2,1)S(1)}, u32[]{:S(2)}, u32[]{:S(2)}) collective-permute-start(bf16[448,256]{1,0:T(8,128)(2,1)S(1)} %finish.3.own), channel_id=1, source_target_pairs={{0,1},{1,0},{2,3},{3,2},{4,5},{5,4},{6,7},{7,6},{8,9},{9,8},{10,11... | collective-permute-start | bytes 688136 | tf_op jit(solution)/shard_map/ppermute | solution.py:301
  38.4 1.1 %collective-permute-done.5.far = bf16[448,256]{1,0:T(8,128)(2,1)S(1)} collective-permute-done((bf16[448,256]{1,0:T(8,128)(2,1)S(1)}, bf16[448,256]{1,0:T(8,128)(2,1)S(1)}, u32[]{:S(2)}, u32[]{:S(2)}) %collective-permute-start.5) | collective-permute-done | bytes 229408 | tf_op jit(solution)/shard_map/ppermute | solution.py:301
  39.5 2.3 %mix.1 = bf16[448,2048]{1,0:T(8,128)(2,1)} custom-call(bf16[448,256]{1,0:T(8,128)(2,1)S(1)} %finish.3.own, bf16[448,256]{1,0:T(8,128)(2,1)S(1)} %collective-permute-done.5.far, f32[2,512]{1,0:T(2,128)S(1)} %copy-done.3, f32[2,512]{1,0:T(2,128)S(1)} %copy-done.4, bf16[2,512,2048]{2,1,0:T(8,128)(2,1)S(1)} %copy-done, bf16[448,2048]{1,0:T(8,128)(2,1)S(1)} %get-tuple-element.20.state), custom_call_target="tpu_custom_call" | custom-call | tf_op jit(solution)/shard_map/mix/pallas_call | solution.py:312
Async XLA Ops:
  0.0 6.8 %copy-start.7 = (f32[32,512]{1,0:T(8,128)S(1)}, f32[32,512]{1,0:T(8,128)}, u32[]{:S(2)}) copy-start(f32[32,512]{1,0:T(8,128)} %constant.32.clone.refs_11_) | copy-start | bytes 196612
  0.0 6.8 %copy-start.8 = (f32[32,512]{1,0:T(8,128)S(1)}, f32[32,512]{1,0:T(8,128)}, u32[]{:S(2)}) copy-start(f32[32,512]{1,0:T(8,128)} %constant.31.clone.refs_10_) | copy-start | bytes 196612
  0.0 6.8 %copy-start.9 = (f32[32,512]{1,0:T(8,128)S(1)}, f32[32,512]{1,0:T(8,128)}, u32[]{:S(2)}) copy-start(f32[32,512]{1,0:T(8,128)} %constant.28.clone.refs_7_) | copy-start | bytes 196612
  0.0 6.8 %copy-start.10 = (f32[32,512]{1,0:T(8,128)S(1)}, f32[32,512]{1,0:T(8,128)}, u32[]{:S(2)}) copy-start(f32[32,512]{1,0:T(8,128)} %constant.27.clone.refs_6_) | copy-start | bytes 196612
  0.0 6.8 %copy-start.11 = (f32[32,512]{1,0:T(8,128)S(1)}, f32[32,512]{1,0:T(8,128)}, u32[]{:S(2)}) copy-start(f32[32,512]{1,0:T(8,128)} %constant.25.clone.refs_3_) | copy-start | bytes 196612
  0.0 6.8 %copy-start.12 = (f32[32,512]{1,0:T(8,128)S(1)}, f32[32,512]{1,0:T(8,128)}, u32[]{:S(2)}) copy-start(f32[32,512]{1,0:T(8,128)} %constant.24.clone.refs_2_) | copy-start | bytes 196612
  0.0 6.8 %copy-start.13 = (f32[14,512]{1,0:T(8,128)S(1)}, f32[14,512]{1,0:T(8,128)}, u32[]{:S(2)}) copy-start(f32[14,512]{1,0:T(8,128)} %constant.30.clone.refs_9_) | copy-start | bytes 86020
  0.1 6.8 %copy-start.14 = (f32[14,512]{1,0:T(8,128)S(1)}, f32[14,512]{1,0:T(8,128)}, u32[]{:S(2)}) copy-start(f32[14,512]{1,0:T(8,128)} %constant.29.clone.refs_8_) | copy-start | bytes 86020
  0.1 6.8 %copy-start.15 = (f32[16,512]{1,0:T(8,128)S(1)}, f32[16,512]{1,0:T(8,128)}, u32[]{:S(2)}) copy-start(f32[16,512]{1,0:T(8,128)} %constant.26.clone.refs_5_) | copy-start | bytes 98308
  0.1 6.8 %copy-start.16 = (f32[16,512]{1,0:T(8,128)S(1)}, f32[16,512]{1,0:T(8,128)}, u32[]{:S(2)}) copy-start(f32[16,512]{1,0:T(8,128)} %constant.23.clone.refs_1_.refs_4_) | copy-start | bytes 98308
  0.1 6.8 %copy-start.17 = (f32[16,512]{1,0:T(8,128)S(1)}, f32[16,512]{1,0:T(8,128)}, u32[]{:S(2)}) copy-start(f32[16,512]{1,0:T(8,128)} %constant.22.clone.refs_0_) | copy-start | bytes 98308
  0.1 6.8 %copy-start.6 = (bf16[2,512,256]{2,1,0:T(8,128)(2,1)S(1)}, bf16[2,512,256]{2,1,0:T(8,128)(2,1)}, u32[]{:S(2)}) copy-start(bf16[2,512,256]{2,1,0:T(8,128)(2,1)} %refs_12_.1) | copy-start | bytes 1572868
  3.6 10.2 %collective-permute-start.1 = (bf16[448,256]{1,0:T(8,128)(2,1)S(1)}, bf16[448,256]{1,0:T(8,128)(2,1)S(1)}, u32[]{:S(2)}, u32[]{:S(2)}) collective-permute-start(bf16[448,256]{1,0:T(8,128)(2,1)S(1)} %first_gate.1.refs_13_.gated), channel_id=1, source_target_pairs={{0,2},{2,4},{4,6},{6,8},{8,10},{10,12},{12,14},{14,16},{16,18},{18... | collective-permute-start | bytes 688136 | tf_op jit(solution)/shard_map/ppermute | solution.py:18
  9.0 4.9 %copy-start.5 = (f32[2,256]{1,0:T(2,128)S(1)}, f32[2,256]{1,0:T(2,128)}, u32[]{:S(2)}) copy-start(f32[2,256]{1,0:T(2,128)} %refs_4_.4) | copy-start | bytes 6148
  9.0 4.5 %collective-permute-start = (bf16[64,256]{1,0:T(8,128)(2,1)S(1)}, bf16[64,256]{1,0:T(8,128)(2,1)S(1)}, u32[]{:S(2)}, u32[]{:S(2)}) collective-permute-start(bf16[64,256]{1,0:T(8,128)(2,1)S(1)} %get-tuple-element.17), channel_id=1, source_target_pairs={{0,4},{2,6},{4,8},{6,10},{8,12},{10,14},{12,16},{14,18},{16,20},{1... | collective-permute-start | bytes 98312 | tf_op jit(solution)/shard_map/ppermute | solution.py:18
  13.9 6.2 %copy-start = (bf16[2,512,2048]{2,1,0:T(8,128)(2,1)S(1)}, bf16[2,512,2048]{2,1,0:T(8,128)(2,1)}, u32[]{:S(2)}) copy-start(bf16[2,512,2048]{2,1,0:T(8,128)(2,1)} %w_out.3) | copy-start | bytes 12582916
  13.9 6.2 %copy-start.1 = (bf16[448,2048]{1,0:T(8,128)(2,1)S(1)}, bf16[448,2048]{1,0:T(8,128)(2,1)}, u32[]{:S(2)}) copy-start(bf16[448,2048]{1,0:T(8,128)(2,1)} %state.1) | copy-start | bytes 5505028
  13.9 6.2 %copy-start.2 = (f32[2,2048]{1,0:T(2,128)S(1)}, f32[2,2048]{1,0:T(2,128)}, u32[]{:S(2)}) copy-start(f32[2,2048]{1,0:T(2,128)} %gain.1) | copy-start | bytes 49156
  13.9 6.2 %copy-start.3 = (f32[2,512]{1,0:T(2,128)S(1)}, f32[2,512]{1,0:T(2,128)}, u32[]{:S(2)}) copy-start(f32[2,512]{1,0:T(2,128)} %ch_gain.3) | copy-start | bytes 12292
  13.9 6.2 %copy-start.4 = (f32[2,512]{1,0:T(2,128)S(1)}, f32[2,512]{1,0:T(2,128)}, u32[]{:S(2)}) copy-start(f32[2,512]{1,0:T(2,128)} %ch_shift.3) | copy-start | bytes 12292
  16.7 3.4 %collective-permute-start.2 = (bf16[448,256]{1,0:T(8,128)(2,1)S(1)}, bf16[448,256]{1,0:T(8,128)(2,1)S(1)}, u32[]{:S(2)}, u32[]{:S(2)}) collective-permute-start(bf16[448,256]{1,0:T(8,128)(2,1)S(1)} %finish.2.own), channel_id=1, source_target_pairs={{0,1},{1,0},{2,3},{3,2},{4,5},{5,4},{6,7},{7,6},{8,9},{9,8},{10,11... | collective-permute-start | bytes 688136 | tf_op jit(solution)/shard_map/ppermute | solution.py:301
  23.2 10.7 %collective-permute-start.4 = (bf16[448,256]{1,0:T(8,128)(2,1)S(1)}, bf16[448,256]{1,0:T(8,128)(2,1)S(1)}, u32[]{:S(2)}, u32[]{:S(2)}) collective-permute-start(bf16[448,256]{1,0:T(8,128)(2,1)S(1)} %get-tuple-element.18.gated), channel_id=1, source_target_pairs={{0,2},{2,4},{4,6},{6,8},{8,10},{10,12},{12,14},{14,16},{16,18},{18... | collective-permute-start | bytes 688136 | tf_op jit(solution)/shard_map/ppermute | solution.py:18
  25.5 3.9 %collective-permute-start.3 = (bf16[64,256]{1,0:T(8,128)(2,1)S(1)}, bf16[64,256]{1,0:T(8,128)(2,1)S(1)}, u32[]{:S(2)}, u32[]{:S(2)}) collective-permute-start(bf16[64,256]{1,0:T(8,128)(2,1)S(1)} %get-tuple-element.19), channel_id=1, source_target_pairs={{0,4},{2,6},{4,8},{6,10},{8,12},{10,14},{12,16},{14,18},{16,20},{1... | collective-permute-start | bytes 98312 | tf_op jit(solution)/shard_map/ppermute | solution.py:18
  36.7 2.8 %collective-permute-start.5 = (bf16[448,256]{1,0:T(8,128)(2,1)S(1)}, bf16[448,256]{1,0:T(8,128)(2,1)S(1)}, u32[]{:S(2)}, u32[]{:S(2)}) collective-permute-start(bf16[448,256]{1,0:T(8,128)(2,1)S(1)} %finish.3.own), channel_id=1, source_target_pairs={{0,1},{1,0},{2,3},{3,2},{4,5},{5,4},{6,7},{7,6},{8,9},{9,8},{10,11... | collective-permute-start | bytes 688136 | tf_op jit(solution)/shard_map/ppermute | solution.py:301
